TPU v7x, 512 devices: a 8x2x16 block of a 8x8x16 slice. The times are simulated.
512 devices in a mesh: grp: 2 (over y), dp: 8 (over x), kv: 16 (over z), tp: 2 (over core).
Axes of the slice: x: 8, y: 2, z: 16, core: 2. Of those that a mesh axis runs over, the one named last changes fastest.
The devices are a block of a 8x8x16 slice.
Arguments:
- tokens: bfloat16 [512, 2048], P(('grp', 'dp'), ('kv', 'tp')), parts along dimension 0, may hold values from -40 to 40
- past_state: float32 [512, 16, 128, 128], P(('grp', 'dp', 'kv'), 'tp'), parts along dimension 0, may hold values from -4 to 4
- mix_gain: float32 [2048], P('kv'), may hold values from 0.1 to 1.9
- w_query: bfloat16 [2048, 2048], P('kv', 'tp'), may hold values from -0.125 to 0.125
- w_forget: bfloat16 [2048, 2048], P('kv', 'tp'), may hold values from -0.125 to 0.125
- w_value: bfloat16 [2048, 2048], P('kv', 'tp'), may hold values from -0.125 to 0.125
- w_gate_out: bfloat16 [2048, 2048], P('kv', 'tp'), may hold values from -0.125 to 0.125
- floor_logits: float32 [2048], P('tp'), may hold values from -6 to 6
- head_gain: float32 [128], replicated, may hold values from 0.1 to 1.9
- w_out: bfloat16 [2048, 2048], P(None, ('kv', 'tp')), may hold values from -0.125 to 0.125
- mlp_gain: float32 [2048], replicated, may hold values from 0.1 to 1.9
- w_gate: bfloat16 [2048, 5632], P(None, ('kv', 'tp')), may hold values from -0.125 to 0.125
- w_up: bfloat16 [2048, 5632], P(None, ('kv', 'tp')), may hold values from -0.125 to 0.125
- w_down: bfloat16 [5632, 2048], P(('kv', 'tp')), may hold values from -0.15625 to 0.15625
Outputs:
- result: bfloat16 [512, 2048], P(('grp', 'dp'), ('kv', 'tp')), parts along dimension 0
- new_state: float32 [512, 16, 128, 128], P(('grp', 'dp', 'kv'), 'tp'), parts along dimension 0
There are 2 independent parts, one for each index of `grp`. A program takes and returns all parts, laid end to end along the dimension named above; an argument that names none is the same for every part. Nothing has to cross between parts.
All inputs are finite; a program needn't handle non-finite values.
Results may differ from a plain program's by a relative error of at most 0.0091.
Values may be sent and summed in bfloat16 or wider, within the bound.
A program may use at most 64 MiB of HBM per device.

v0:
```python
import jax
import jax.numpy as jnp
from jax import lax
from jax.sharding import PartitionSpec as P

D = 2048
DK = 128
DV = 128


epsilon = 1e-06


def in_order(pieces, dim):
    pieces = jnp.moveaxis(pieces, 0, dim)
    lengths = pieces.shape
    return pieces.reshape(*lengths[:dim], lengths[dim] * lengths[dim + 1], *lengths[dim + 2 :])


def from_everyone(x, axis):
    length = lax.axis_size(axis)
    return lax.all_to_all(jnp.broadcast_to(x[None], (length, *x.shape)), axis, 0, 0, tiled=True)


def gathered_copies(x, axis, dim):
    return in_order(from_everyone(x, axis), dim)


def over_copies(x, axis):
    return from_everyone(x, axis).sum(axis=0)


def cut_along(x, dim, length):
    lengths = x.shape
    pieces = x.reshape(*lengths[:dim], length, lengths[dim] // length, *lengths[dim + 1 :])
    return jnp.moveaxis(pieces, dim, 0)


def sent_and_summed(x, axis, dim):
    length = lax.axis_size(axis)
    pieces = lax.all_to_all(cut_along(x, dim, length), axis, 0, 0, tiled=True)
    return jnp.sum(pieces.astype(jnp.float32), axis=0)


def sent_together(arrays, axis, dim, along):
    ends, at = ([], 0)
    for a in arrays[:-1]:
        at += a.shape[along]
        ends.append(at)
    both = jnp.concatenate(arrays, axis=along)
    return tuple(jnp.split(sent_and_summed(both, axis, dim), ends, axis=along))


def summed_on_arrival(x, axis, dim):
    pieces = cut_along(x, dim, lax.axis_size(axis))
    arrived = lax.all_to_all(pieces, axis, split_axis=0, concat_axis=0, tiled=True)
    return arrived.sum(axis=0)


def body(
    tokens,
    past_state,
    mix_gain,
    w_query,
    w_forget,
    w_value,
    w_gate_out,
    floor_logits,
    head_gain,
    w_out,
    mlp_gain,
    w_gate,
    w_up,
    w_down,
):
    kv_count = lax.axis_size("kv")
    tp_count = lax.axis_size("tp")
    rows_local = past_state.shape[0]
    heads_local = past_state.shape[1]
    width_cols = tokens.shape[1]
    own_block = gathered_copies(tokens, "tp", 1)
    block_f = own_block.astype(jnp.float32)
    square_rows = over_copies(jnp.sum(block_f * block_f, axis=1), "kv")
    gained = (own_block.astype(jnp.float32) * mix_gain).astype(jnp.bfloat16)
    mine = lax.dynamic_slice_in_dim(square_rows, lax.axis_index("kv") * rows_local, rows_local, 0)
    row_scale = lax.rsqrt(mine / D + epsilon)[:, None]
    query_sum, forget_sum, value_sum, gate_sum = sent_together(
        (
            jnp.dot(gained, w_query, preferred_element_type=jnp.float32).astype(jnp.bfloat16),
            jnp.dot(gained, w_forget, preferred_element_type=jnp.float32).astype(jnp.bfloat16),
            jnp.dot(gained, w_value, preferred_element_type=jnp.float32).astype(jnp.bfloat16),
            jnp.dot(gained, w_gate_out, preferred_element_type=jnp.float32).astype(jnp.bfloat16),
        ),
        "kv",
        0,
        1,
    )
    query = query_sum * row_scale
    forget_pre = forget_sum * row_scale
    value = value_sum * row_scale
    gate_pre = gate_sum * row_scale
    lower = jax.nn.sigmoid(floor_logits).reshape(heads_local, DK)
    forget = lower + (1.0 - lower) * jax.nn.sigmoid(forget_pre.reshape(rows_local, heads_local, DK))
    values = value.reshape(rows_local, heads_local, DV)
    new_state = forget[..., None] * past_state + (1.0 - forget)[..., None] * values[:, :, None, :]
    activ = jax.nn.silu(query.reshape(rows_local, heads_local, DK))
    head_out = jnp.einsum("shkv,shk->shv", new_state, activ, precision=lax.Precision.HIGHEST)
    normed = head_out * lax.rsqrt(jnp.mean(head_out * head_out, axis=2, keepdims=True) + epsilon)
    normed = normed * head_gain * jax.nn.silu(gate_pre.reshape(rows_local, heads_local, DV))
    mixed = normed.reshape(1, rows_local, heads_local * DV).astype(jnp.bfloat16)
    every_head = gathered_copies(mixed, ("kv", "tp"), 0)
    every_head = every_head.reshape(kv_count, tp_count, rows_local, heads_local * DV)
    out_blocks = w_out.reshape(tp_count, heads_local * DV, width_cols)
    projected = jnp.einsum(
        "ktsh,thc->ksc", every_head, out_blocks, preferred_element_type=jnp.float32
    )
    middle = (
        tokens.astype(jnp.float32) + projected.reshape(kv_count * rows_local, width_cols)
    ).astype(jnp.bfloat16)
    gathered = gathered_copies(middle, ("kv", "tp"), 1)
    gathered_f = gathered.astype(jnp.float32)
    mlp_scale = lax.rsqrt(jnp.mean(gathered_f * gathered_f, axis=1, keepdims=True) + epsilon)
    mlp_in = (gathered_f * mlp_scale * mlp_gain).astype(jnp.bfloat16)
    gate = jnp.dot(mlp_in, w_gate, preferred_element_type=jnp.float32)
    upward = jnp.dot(mlp_in, w_up, preferred_element_type=jnp.float32)
    hidden = (jax.nn.silu(gate) * upward).astype(jnp.bfloat16)
    terms = jnp.dot(hidden, w_down, preferred_element_type=jnp.float32)
    summed = summed_on_arrival(terms, ("kv", "tp"), 1)
    result = (middle.astype(jnp.float32) + summed).astype(jnp.bfloat16)
    return (result, new_state)


def solution(mesh):
    placed = (
        P(("grp", "dp"), ("kv", "tp")),
        P(("grp", "dp", "kv"), "tp", None, None),
        P("kv"),
        P("kv", "tp"),
        P("kv", "tp"),
        P("kv", "tp"),
        P("kv", "tp"),
        P("tp"),
        P(),
        P(None, ("kv", "tp")),
        P(),
        P(None, ("kv", "tp")),
        P(None, ("kv", "tp")),
        P(("kv", "tp"), None),
    )
    return jax.shard_map(
        body,
        mesh=mesh,
        in_specs=placed,
        out_specs=(P(("grp", "dp"), ("kv", "tp")), P(("grp", "dp", "kv"), "tp", None, None)),
        check_vma=False,
    )
```

profile of v0, /device:TPU:65, one launch (start us, length us, event | category | flops | bytes accessed | tf_op | source)
XLA Modules:
  0.0 163.1 jit_solution(3353764215756485367)
XLA Ops:
  0.7 0.8 broadcast_in_dim.8
  1.5 44.8 %all_to_all.31 = bf16[2,2,1024]{2,1,0:T(2,128)(2,1)S(1)} all-to-all(bf16[2,2,1024]{2,1,0:T(2,128)(2,1)S(1)} %reshape.106), channel_id=1, replica_groups=mesh['grp'=2,'dp'=8,'kv'=16,'tp'=2] {'tp'}, dimensions={0} | all-to-all | bytes 16384 | tf_op jit(solution)/shard_map/all_to_all | solution.py:22
  46.5 0.6 broadcast_in_dim.9
  47.2 4.0 %all-to-all-start.2 = ((f32[16,1,32]{2,1,0:T(1,128)}), f32[16,1,32]{2,1,0:T(1,128)S(1)}, u32[]{:S(2)}, u32[]{:S(2)}) async-start(f32[16,1,32]{2,1,0:T(1,128)} %broadcast_in_dim.9), calls=%async_computation.2 | async-start | bytes 16384 | tf_op jit(solution)/shard_map/all_to_all | solution.py:22
  51.5 0.6 copy-done.6
  52.5 0.6 copy-done.8
  53.3 0.9 reshape.96
  54.2 7.8 %all-to-all-done.2 = f32[16,1,32]{2,1,0:T(1,128)S(1)} async-done(((f32[16,1,32]{2,1,0:T(1,128)}), f32[16,1,32]{2,1,0:T(1,128)S(1)}, u32[]{:S(2)}, u32[]{:S(2)}) %all-to-all-start.2) | async-done | bytes 2080 | tf_op jit(solution)/shard_map/all_to_all | solution.py:22
  62.0 4.0 %all-to-all-start.1 = ((bf16[16,2,4096]{2,1,0:T(2,128)(2,1)}), bf16[16,2,4096]{2,1,0:T(2,128)(2,1)S(1)}, u32[]{:S(2)}, u32[]{:S(2)}) async-start(bf16[16,2,4096]{2,1,0:T(2,128)(2,1)} %reshape.96), calls=%async_computation.1 | async-start | bytes 524288 | tf_op jit(solution)/shard_map/all_to_all | solution.py:41
  66.0 0.7 copy-done.12
  66.8 11.6 %all-to-all-done.1 = bf16[16,2,4096]{2,1,0:T(2,128)(2,1)S(1)} async-done(((bf16[16,2,4096]{2,1,0:T(2,128)(2,1)}), bf16[16,2,4096]{2,1,0:T(2,128)(2,1)S(1)}, u32[]{:S(2)}, u32[]{:S(2)}) %all-to-all-start.1) | async-done | bytes 262176 | tf_op jit(solution)/shard_map/all_to_all | solution.py:41
  78.7 0.6 multiply_add_fusion
  79.3 1.0 fusion.35
  80.5 0.7 copy-done.14
  81.3 28.0 %all_to_all.32 = bf16[32,1,2,1024]{3,2,1,0:T(2,128)(2,1)S(1)} all-to-all(bf16[32,1,2,1024]{3,2,1,0:T(2,128)(2,1)S(1)} %broadcast_in_dim.10), channel_id=1, replica_groups=mesh['grp'=2,'dp'=8,'kv'=16,'tp'=2] {'kv','tp'}, dimensions={0} | all-to-all | bytes 262144 | tf_op jit(solution)/shard_map/all_to_all | solution.py:22
  109.4 0.8 copy-done.9
  110.7 20.4 %all_to_all.33 = bf16[32,2,1024]{2,1,0:T(2,128)(2,1)S(1)} all-to-all(bf16[32,2,1024]{2,1,0:T(2,128)(2,1)S(1)} %reshape.108), channel_id=1, replica_groups=mesh['grp'=2,'dp'=8,'kv'=16,'tp'=2] {'kv','tp'}, dimensions={0} | all-to-all | bytes 262144 | tf_op jit(solution)/shard_map/all_to_all | solution.py:22
  132.1 0.6 copy-done.3
  132.7 0.3 fusion.33
  133.1 0.7 fusion.1
  134.7 25.8 %all_to_all.34 = f32[32,1,2048]{2,1,0:T(1,128)S(1)} all-to-all(f32[32,1,2048]{2,1,0:T(1,128)S(1)} %reshape.110), channel_id=1, replica_groups=mesh['grp'=2,'dp'=8,'kv'=16,'tp'=2] {'kv','tp'}, dimensions={0} | all-to-all | bytes 524288 | tf_op jit(solution)/shard_map/all_to_all | solution.py:56
  160.4 0.5 broadcast.118
  161.0 1.3 reduce.5
  162.5 0.6 add_convert_fusion
  (65 shorter events, 4.5 us)
Async XLA Ops:
  0.6 132.4 %copy-start = (bf16[176,2048]{1,0:T(8,128)(2,1)S(1)}, bf16[176,2048]{1,0:T(8,128)(2,1)}, u32[]{:S(2)}) copy-start(bf16[176,2048]{1,0:T(8,128)(2,1)} %param.27) | copy-start | bytes 2162692
  0.6 50.7 %copy-start.5 = (bf16[128,1024]{1,0:T(8,128)(2,1)S(1)}, bf16[128,1024]{1,0:T(8,128)(2,1)}, u32[]{:S(2)}) copy-start(bf16[128,1024]{1,0:T(8,128)(2,1)} %param.20) | copy-start | bytes 786436
  47.2 4.2 %copy-start.13 = (f32[128]{0:T(128)S(1)}, f32[128]{0:T(128)}, u32[]{:S(2)}) copy-start(f32[128]{0:T(128)} %param.16) | copy-start | bytes 1540
  47.2 14.9 %all-to-all-start.2 = ((f32[16,1,32]{2,1,0:T(1,128)}), f32[16,1,32]{2,1,0:T(1,128)S(1)}, u32[]{:S(2)}, u32[]{:S(2)}) async-start(f32[16,1,32]{2,1,0:T(1,128)} %broadcast_in_dim.9), calls=%async_computation.2 | async-start | bytes 16384 | tf_op jit(solution)/shard_map/all_to_all | solution.py:22
  51.2 1.0 copy-start.6
  51.4 1.0 copy-start.7
  52.2 1.0 copy-start.8
  53.3 25.4 %copy-start.2 = (f32[2,8,128,128]{3,2,1,0:T(8,128)S(1)}, f32[2,8,128,128]{3,2,1,0:T(8,128)}, u32[]{:S(2)}) copy-start(f32[2,8,128,128]{3,2,1,0:T(8,128)} %param.15) | copy-start | bytes 3145732
  62.0 16.4 %all-to-all-start.1 = ((bf16[16,2,4096]{2,1,0:T(2,128)(2,1)}), bf16[16,2,4096]{2,1,0:T(2,128)(2,1)S(1)}, u32[]{:S(2)}, u32[]{:S(2)}) async-start(bf16[16,2,4096]{2,1,0:T(2,128)(2,1)} %reshape.96), calls=%async_computation.1 | async-start | bytes 524288 | tf_op jit(solution)/shard_map/all_to_all | solution.py:41
  66.0 0.7 copy-start.12
  79.3 31.1 %copy-start.1 = (f32[2,8,128,128]{3,2,1,0:T(8,128)}, f32[2,8,128,128]{3,2,1,0:T(8,128)S(1)}, u32[]{:S(2)}) copy-start(f32[2,8,128,128]{3,2,1,0:T(8,128)S(1)} %multiply_add_fusion) | copy-start | bytes 3145732
  80.4 0.7 copy-start.14
  109.3 1.0 copy-start.9
  109.4 0.9 copy-start.11
  131.6 1.1 copy-start.3
  131.9 0.8 copy-start.10
  131.9 1.2 copy-start.4
where the time goes:
time: 164 us; the launch traced here: 163 us
  blocking collectives  119 us (73%)
  waiting for transfers between devices  19.3 us (12%)
  local copies, waits for them, and re-layouts  9.4 us (6%)
  starting transfers between devices  8.02 us (5%)
  other arithmetic  3.52 us (2%)
  matrix products  2.86 us (2%)
    all_to_all x3, blocking collectives, from_everyone(): lax.all_to_all(jnp.broadcast_to(x[None], (length, *x.shape)), axis, 0, 0,...  93.2 us
    all_to_all x1, blocking collectives, summed_on_arrival(): lax.all_to_all(pieces, axis, split_axis=0, concat_axis=0, tiled=True)  25.8 us
    all_to_all x1, waiting for transfers between devices, sent_and_summed(): pieces = lax.all_to_all(cut_along(x, dim, length), axis, 0, 0, tiled=True)  11.6 us
    all_to_all x1, waiting for transfers between devices, from_everyone(): lax.all_to_all(jnp.broadcast_to(x[None], (length, *x.shape)), axis, 0, 0,...  7.79 us
    unnamed x38, local copies, waits for them, and re-layouts  5.21 us
    all_to_all x1, starting transfers between devices, from_everyone(): lax.all_to_all(jnp.broadcast_to(x[None], (length, *x.shape)), axis, 0, 0,...  4.04 us
    all_to_all x1, starting transfers between devices, sent_and_summed(): pieces = lax.all_to_all(cut_along(x, dim, length), axis, 0, 0, tiled=True)  3.98 us
  transfers between devices with their start and end apart: 2, of which 2 were waited for; matrix products, arithmetic and copies ran while one was open for 1% of the time, Pallas kernels for 0%

commit v1 on v0

v1 whole, which is shorter than its diff:
```python
import functools

import jax
import jax.numpy as jnp
from jax import lax
from jax.experimental import pallas as pl
from jax.experimental.pallas import tpu as pltpu
from jax.sharding import PartitionSpec as P

MESH = pl.DeviceIdType.MESH
EPS = 1e-06
F32 = jnp.float32
BF16 = jnp.bfloat16


def dot(a, b):
    return jnp.dot(a, b, preferred_element_type=F32)


def packed(x):
    half = x.shape[0] // 2
    return jnp.concatenate([x[:half], x[half:]], axis=1)


def halves_swapped(x):
    return pltpu.roll(x, x.shape[1] // 2, 1)


def kernel(
    kv,
    tp,
    tokens,
    past_state,
    mix_gain,
    w_query,
    w_forget,
    w_value,
    w_gate_out,
    floor_logits,
    head_gain,
    w_out,
    mlp_gain,
    w_gate,
    w_up,
    w_down,
    result,
    new_state,
    tok_other,
    proj_w,
    state,
    out_w,
    mlp_w,
    down_w,
    floors,
    heads,
    chunk_out,
    chunk_in,
    sq_out,
    sq_in,
    mix,
    part_out,
    part_in,
    mid,
    wide_out,
    wide_in,
    terms_out,
    terms_in,
    local_sem,
    pair_send,
    pair_recv,
    rs_send,
    rs_recv,
    sq_send,
    sq_recv,
    mix_send,
    mix_recv,
    mid_send,
    mid_recv,
    term_send,
    term_recv,
):
    z = lax.axis_index("kv")
    c = lax.axis_index("tp")
    other = 1 - c
    rows, feats = tokens.shape
    seqs, heads_local, dk, dv = past_state.shape
    units = w_gate.shape[3]
    group = heads_local * seqs
    half_rows = rows // 2
    width = kv * tp * feats
    half_kv = kv // tp
    half_cols = half_kv * tp * feats

    def local(src, dst, i):
        copy = pltpu.make_async_copy(src, dst, local_sem.at[i])
        copy.start()
        return copy

    def remote(src, dst, send, recv, to_z, to_c):
        return pltpu.make_async_remote_copy(
            src_ref=src,
            dst_ref=dst,
            send_sem=send,
            recv_sem=recv,
            device_id={"kv": to_z, "tp": to_c},
            device_id_type=MESH,
        )

    def peer(d):
        return lax.rem(z + d, kv)

    far_first = sorted(range(1, kv), key=lambda d: -min(d, kv - d))
    near_first = far_first[::-1]

    barrier = pltpu.get_barrier_semaphore()
    for d in far_first:
        pl.semaphore_signal(barrier, inc=1, device_id={"kv": peer(d), "tp": c}, device_id_type=MESH)
    pl.semaphore_signal(barrier, inc=1, device_id={"kv": z, "tp": other}, device_id_type=MESH)

    proj_copies = [
        local(w, proj_w.at[i], i) for i, w in enumerate((w_query, w_forget, w_value, w_gate_out))
    ]
    state_copy = local(past_state, state, 4)
    half_of = pl.ds(pl.multiple_of(c * half_cols, half_cols), half_cols)
    half_of_other = pl.ds(pl.multiple_of(other * half_cols, half_cols), half_cols)
    weight_copies = [
        local(w_out.at[c], out_w.at[0], 5),
        local(w_gate.at[:, c], mlp_w.at[0], 6),
        local(w_up.at[:, c], mlp_w.at[2], 7),
        local(w_down.at[:, half_of], down_w.at[0], 8),
    ]

    r = lax.broadcasted_iota(jnp.int32, (kv * group, kv * group), 0)
    col = lax.broadcasted_iota(jnp.int32, (kv * group, kv * group), 1)
    s_of = lax.rem(r, seqs)
    to_chunks = lax.rem(r // seqs, heads_local) * (kv * seqs) + (r // group) * seqs + s_of
    spread = jnp.where(col == to_chunks, 1.0, 0.0).astype(BF16)
    to_heads = lax.rem(r // seqs, kv) * group + (r // (kv * seqs)) * seqs + s_of
    gather = jnp.where(col == to_heads, 1.0, 0.0).astype(BF16)

    lower_in = jax.nn.sigmoid(floor_logits[...])
    for h in range(heads_local):
        floors[pl.ds(h * seqs, seqs), :] = jnp.broadcast_to(lower_in[h : h + 1], (seqs, dk))

    pl.semaphore_wait(barrier, kv)

    tok = remote(tokens, tok_other, pair_send.at[0], pair_recv.at[0], z, other)
    tok.start()
    lane = lax.broadcasted_iota(jnp.int32, (1, tp * feats), 1)
    low = lane < feats
    own = tokens[...].astype(F32)
    own_twice = jnp.concatenate([own, own], axis=1)
    tok.wait_recv()
    got = tok_other[...].astype(F32)
    got_twice = jnp.concatenate([got, got], axis=1)
    mine = lax.broadcasted_iota(jnp.int32, (rows, tp * feats), 1) // feats == c
    block = jnp.where(mine, own_twice, got_twice)
    squares = jnp.sum(block * block, axis=1, keepdims=True)
    sq_out[...] = jnp.broadcast_to(squares, (rows, dk)).reshape(kv, seqs, dk)
    gained = (block * mix_gain[...]).astype(BF16)
    for i in range(4):
        proj_copies[i].wait()
        product = dot(gained, proj_w[i]).astype(BF16)
        stack = jnp.concatenate([product[:, h * dk : (h + 1) * dk] for h in range(heads_local)], axis=0)
        ordered = dot(spread, stack).astype(BF16)
        chunk_out[:, pl.ds(i * group, group), :] = ordered.reshape(kv, group, dk)

    rs, sq = {}, {}
    for d in far_first:
        to = peer(d)
        rs[d] = remote(chunk_out.at[to], chunk_in.at[d], rs_send.at[d], rs_recv.at[d], to, c)
        sq[d] = remote(sq_out.at[to], sq_in.at[d], sq_send.at[d], sq_recv.at[d], to, c)
        sq[d].start()
        rs[d].start()
    swaps = [
        remote(w_out.at[other], out_w.at[1], pair_send.at[1], pair_recv.at[1], z, other),
        remote(w_gate.at[:, other], mlp_w.at[1], pair_send.at[2], pair_recv.at[2], z, other),
        remote(w_up.at[:, other], mlp_w.at[3], pair_send.at[3], pair_recv.at[3], z, other),
        remote(w_down.at[:, half_of_other], down_w.at[1], pair_send.at[4], pair_recv.at[4], z, other),
    ]
    for s in swaps:
        s.start()

    total_sq = sq_out[z]
    total = chunk_out[z].astype(F32)
    for d in near_first:
        sq[d].wait_recv()
        total_sq = total_sq + sq_in[d]
        rs[d].wait_recv()
        total = total + chunk_in[d].astype(F32)

    scale_s = lax.rsqrt(total_sq / width + EPS)
    row_of = lax.broadcasted_iota(jnp.int32, (group, dk), 0)
    scale = jnp.broadcast_to(scale_s[0:1], (group, dk))
    for s in range(1, seqs):
        scale = jnp.where(lax.rem(row_of, seqs) == s, jnp.broadcast_to(scale_s[s : s + 1], (group, dk)), scale)
    query = total[0:group] * scale
    forget_pre = total[group : 2 * group] * scale
    value = total[2 * group : 3 * group] * scale
    gate_pre = total[3 * group : 4 * group] * scale
    lower = floors[...]
    forget = lower + (1.0 - lower) * jax.nn.sigmoid(forget_pre)
    activ = query * jax.nn.sigmoid(query)
    columns = jnp.concatenate([forget, activ, jnp.zeros((dk - 2 * group, dk), F32)], axis=0).T

    state_copy.wait()
    for h in range(heads_local):
        for s in range(seqs):
            i = h * seqs + s
            v_row = value[i : i + 1]
            f_col = columns[:, i : i + 1]
            q_col = columns[:, group + i : group + i + 1]
            new = v_row + f_col * (state[s, h] - v_row)
            state[s, h] = new
            heads[pl.ds(i, 1), :] = jnp.sum(new * q_col, axis=0, keepdims=True)
    state_out = pltpu.make_async_copy(state, new_state, local_sem.at[4])
    state_out.start()

    head_out = heads[...]
    normed = head_out * lax.rsqrt(jnp.mean(head_out * head_out, axis=1, keepdims=True) + EPS)
    mixed = normed * head_gain[...] * (gate_pre * jax.nn.sigmoid(gate_pre))
    mix[z] = mixed.astype(BF16)
    ag = {}
    for d in far_first:
        ag[d] = remote(mix.at[z], mix.at[z], mix_send.at[d], mix_recv.at[d], peer(d), c)
        ag[d].start()
    weight_copies[0].wait()
    swaps[0].wait_recv()
    for d in near_first:
        ag[d].wait_recv()
    by_head = dot(gather, mix[...].reshape(kv * group, dv)).astype(BF16)
    every = jnp.concatenate([by_head[h * rows : (h + 1) * rows] for h in range(heads_local)], axis=1)
    part_out[...] = packed(dot(every, out_w[1]))
    part = remote(part_out, part_in, pair_send.at[5], pair_recv.at[5], z, other)
    part.start()
    kept = packed(dot(every, out_w[0])) + packed(own)
    part.wait_recv()
    middle = (kept + part_in[...]).astype(BF16)
    mid[z] = middle
    am = {}
    for d in far_first:
        am[d] = remote(mid.at[z], mid.at[z], mid_send.at[d], mid_recv.at[d], peer(d), c)
        am[d].start()

    gain = mlp_gain[...]
    gain_swapped = halves_swapped(gain)
    first = c == 0
    gain_low = jnp.where(first, gain, gain_swapped)
    gain_high = jnp.where(first, gain_swapped, gain)
    for w in weight_copies[1:]:
        w.wait()
    for s in swaps[1:]:
        s.wait_recv()
    for d in near_first:
        am[d].wait_recv()
    tops, bottoms = [], []
    squares = jnp.zeros((half_rows, tp * feats), F32)
    for i in range(kv // 2):
        a = mid[2 * i].astype(F32)
        b = mid[2 * i + 1].astype(F32)
        squares = squares + a * a + b * b
        g = jnp.where(low, gain_low[2 * i : 2 * i + 1], gain_high[2 * i + 1 : 2 * i + 2])
        tops.append((jnp.where(low, a, halves_swapped(b)) * g).astype(BF16))
        bottoms.append((jnp.where(low, halves_swapped(a), b) * g).astype(BF16))
    features = jnp.concatenate(
        [jnp.concatenate(tops, axis=1), jnp.concatenate(bottoms, axis=1)], axis=0
    )
    sq_top = jnp.sum(jnp.where(low, squares, 0.0), axis=1, keepdims=True)
    sq_bottom = jnp.sum(jnp.where(low, 0.0, squares), axis=1, keepdims=True)
    sq_mid = jnp.concatenate([sq_top, sq_bottom], axis=0)
    sums = []
    for i in range(4):
        sums.append(dot(features, mlp_w[i].reshape(kv * feats, units)))
        wide_out[i, :, pl.ds(0, units)] = sums[i]
    wide_out[4, :, :] = jnp.broadcast_to(sq_mid, wide_out.shape[1:])
    wide = remote(wide_out, wide_in, pair_send.at[6], pair_recv.at[6], z, other)
    wide.start()
    wide.wait_recv()
    mlp_scale = lax.rsqrt((sq_mid + wide_in[4, :, 0:1]) / width + EPS)
    terms = None
    for i in range(2):
        gate = (sums[i] + wide_in[1 - i, :, pl.ds(0, units)]) * mlp_scale
        upward = (sums[2 + i] + wide_in[3 - i, :, pl.ds(0, units)]) * mlp_scale
        hidden = (gate * jax.nn.sigmoid(gate) * upward).astype(BF16)
        term = dot(hidden, down_w[i])
        terms = term if terms is None else terms + term

    sends = []
    for i in range(half_kv):
        at = slice(i * tp * feats, (i + 1) * tp * feats)
        top, bottom = terms[:half_rows, at], terms[half_rows:, at]
        to = c * half_kv + i
        for to_c, message in (
            (0, jnp.where(low, top, halves_swapped(bottom))),
            (1, jnp.where(low, halves_swapped(top), bottom)),
        ):
            n = 2 * i + to_c
            terms_out[n] = message.astype(BF16)
            copy = remote(terms_out.at[n], terms_in.at[z], term_send.at[n], term_recv.at[z], to, to_c)
            to_self = jnp.logical_and(to == z, to_c == c)
            sends.append((copy, to_self, n))

            @pl.when(jnp.logical_not(to_self))
            def _(copy=copy):
                copy.start()

            @pl.when(to_self)
            def _(n=n):
                terms_in[z] = terms_out[n]

    for i in range(kv):
        from_self = jnp.logical_and(i == z, c == z // half_kv)

        @pl.when(jnp.logical_not(from_self))
        def _(i=i):
            remote(terms_out.at[0], terms_in.at[i], term_send.at[0], term_recv.at[i], z, other).wait_recv()

    summed = middle.astype(F32) + jnp.sum(terms_in[...].astype(F32), axis=0)
    result[pl.ds(0, half_rows), :] = summed[:, :feats].astype(BF16)
    result[pl.ds(half_rows, half_rows), :] = summed[:, feats:].astype(BF16)

    tok.wait_send()
    part.wait_send()
    wide.wait_send()
    for s in swaps:
        s.wait_send()
    for d in near_first:
        rs[d].wait_send()
        sq[d].wait_send()
        ag[d].wait_send()
        am[d].wait_send()
    for copy, to_self, n in sends:

        @pl.when(jnp.logical_not(to_self))
        def _(copy=copy):
            copy.wait_send()

    state_out.wait()


def body(
    kv,
    tp,
    tokens,
    past_state,
    mix_gain,
    w_query,
    w_forget,
    w_value,
    w_gate_out,
    floor_logits,
    head_gain,
    w_out,
    mlp_gain,
    w_gate,
    w_up,
    w_down,
):
    rows, feats = tokens.shape
    seqs, heads_local, dk, dv = past_state.shape
    units = w_gate.shape[1]
    group = heads_local * seqs
    channels = heads_local * dv
    half_cols = w_down.shape[1] // tp
    wide = -(-units // 128) * 128
    in_vmem = pl.BlockSpec(memory_space=pltpu.VMEM)
    anywhere = pl.BlockSpec(memory_space=pl.ANY)
    dma = pltpu.SemaphoreType.DMA
    return pl.pallas_call(
        functools.partial(kernel, kv, tp),
        name="decode_step",
        out_shape=(
            jax.ShapeDtypeStruct((rows, feats), BF16),
            jax.ShapeDtypeStruct(past_state.shape, F32),
        ),
        in_specs=[
            in_vmem,
            anywhere,
            in_vmem,
            anywhere,
            anywhere,
            anywhere,
            anywhere,
            in_vmem,
            in_vmem,
            anywhere,
            in_vmem,
            anywhere,
            anywhere,
            anywhere,
        ],
        out_specs=(in_vmem, anywhere),
        scratch_shapes=[
            pltpu.VMEM((rows, feats), BF16),
            pltpu.VMEM((4, *w_query.shape), BF16),
            pltpu.VMEM(past_state.shape, F32),
            pltpu.VMEM((2, channels, feats), BF16),
            pltpu.VMEM((4, kv, feats, units), BF16),
            pltpu.VMEM((2, units, half_cols), BF16),
            pltpu.VMEM((group, dk), F32),
            pltpu.VMEM((group, dv), F32),
            pltpu.VMEM((kv, 4 * group, dk), BF16),
            pltpu.VMEM((kv, 4 * group, dk), BF16),
            pltpu.VMEM((kv, seqs, dk), F32),
            pltpu.VMEM((kv, seqs, dk), F32),
            pltpu.VMEM((kv, group, dv), BF16),
            pltpu.VMEM((rows // 2, 2 * feats), F32),
            pltpu.VMEM((rows // 2, 2 * feats), F32),
            pltpu.VMEM((kv, rows // 2, 2 * feats), BF16),
            pltpu.VMEM((5, rows, wide), F32),
            pltpu.VMEM((5, rows, wide), F32),
            pltpu.VMEM((kv, rows // 2, 2 * feats), BF16),
            pltpu.VMEM((kv, rows // 2, 2 * feats), BF16),
            dma((9,)),
            dma((7,)),
            dma((7,)),
            dma((kv,)),
            dma((kv,)),
            dma((kv,)),
            dma((kv,)),
            dma((kv,)),
            dma((kv,)),
            dma((kv,)),
            dma((kv,)),
            dma((kv,)),
            dma((kv,)),
        ],
        compiler_params=pltpu.CompilerParams(
            collective_id=0, has_side_effects=True, vmem_limit_bytes=32 * 1024 * 1024
        ),
    )(
        tokens,
        past_state,
        mix_gain.reshape(1, -1),
        w_query,
        w_forget,
        w_value,
        w_gate_out,
        floor_logits.reshape(heads_local, dk),
        head_gain.reshape(1, -1),
        w_out.reshape(tp, channels, feats),
        mlp_gain.reshape(kv, tp * feats),
        w_gate.reshape(kv, tp, feats, units),
        w_up.reshape(kv, tp, feats, units),
        w_down,
    )


def solution(mesh):
    placed = (
        P(("grp", "dp"), ("kv", "tp")),
        P(("grp", "dp", "kv"), "tp", None, None),
        P("kv"),
        P("kv", "tp"),
        P("kv", "tp"),
        P("kv", "tp"),
        P("kv", "tp"),
        P("tp"),
        P(),
        P(None, ("kv", "tp")),
        P(),
        P(None, ("kv", "tp")),
        P(None, ("kv", "tp")),
        P(("kv", "tp"), None),
    )
    return jax.shard_map(
        functools.partial(body, mesh.shape["kv"], mesh.shape["tp"]),
        mesh=mesh,
        in_specs=placed,
        out_specs=(P(("grp", "dp"), ("kv", "tp")), P(("grp", "dp", "kv"), "tp", None, None)),
        check_vma=False,
    )
```

time: 164 us -> 104 us (0.63)
  blocking collectives: 119 us -> 0 us
  Pallas kernels: 0 us -> 91.7 us
  waiting for transfers between devices: 19.3 us -> 0 us
  starting transfers between devices: 8.02 us -> 0 us
  other arithmetic: 3.52 us -> 0 us
  matrix products: 2.86 us -> 0 us
    all_to_all x4 -> x0, blocking collectives: 119 us -> none  [the longest x3 93.2 us: from_everyone(): lax.all_to_all(jnp.broadcast_to(x[None], (length, *x.shape)), axis, 0, 0,...]
    pallas_call x0 -> x1, Pallas kernels: none -> 91.7 us  [body(): pl.pallas_call(functools.partial(kernel, kv, tp), name='decode_step', out...]
    all_to_all x2 -> x0, waiting for transfers between devices: 19.3 us -> none  [the longest x1 11.6 us: sent_and_summed(): pieces = lax.all_to_all(cut_along(x, dim, length), axis, 0, 0, tiled=True)]
    all_to_all x2 -> x0, starting transfers between devices: 8.02 us -> none  [the longest x1 4.04 us: from_everyone(): lax.all_to_all(jnp.broadcast_to(x[None], (length, *x.shape)), axis, 0, 0,...]
    unnamed x38 -> x29, local copies, waits for them, and re-layouts: 5.21 us -> 10.5 us
    dot_general x8 -> x0, matrix products: 2.86 us -> none  [the longest x1 1 us: body(): jnp.einsum('shkv,shk->shv', new_state, activ, precision=lax.Precision.HIG...]
  transfers between devices with their start and end apart: 2 -> 0, of which waited for: 2 -> 0; matrix products, arithmetic and copies ran while one was open for 1% -> 0% of each run, Pallas kernels for 0% -> 0%
where the time goes in v1:
time: 104 us; the launch traced here: 103 us
  Pallas kernels  91.7 us (88%)
  local copies, waits for them, and re-layouts  10.5 us (10%)
    pallas_call x1, Pallas kernels, body(): pl.pallas_call(functools.partial(kernel, kv, tp), name='decode_step', out...  91.7 us
    unnamed x29, local copies, waits for them, and re-layouts  10.5 us

profile of v1, /device:TPU:65, one launch (start us, length us, event | category | flops | bytes accessed | tf_op | source)
XLA Modules:
  0.0 103.0 jit_solution(10944179422512117376)
XLA Ops:
  0.6 0.0 copy-start.11
  0.6 1.3 %copy.16 = bf16[2048,64]{1,0:T(8,128)(2,1)S(1)} copy(bf16[2048,64]{0,1:T(8,128)(2,1)} %param.23) | data formatting | bytes 524288 | tf_op args[9]
  1.9 0.0 copy-done.11
  1.9 0.5 copy.17
  2.5 0.0 copy-start.1
  2.5 0.0 copy-start.6
  2.5 0.0 copy-start.7
  2.5 0.0 copy-start.8
  2.5 1.5 %copy.18 = bf16[2048,176]{1,0:T(8,128)(2,1)S(1)} copy(bf16[2048,176]{0,1:T(8,128)(2,1)} %param.26) | data formatting | bytes 1441792 | tf_op args[12]
  4.0 0.0 copy-start.9
  4.0 0.0 copy-start.10
  4.0 0.0 copy-done.1
  4.0 0.0 copy-done.6
  4.0 0.0 copy-done.7
  4.1 0.6 copy-done.9
  4.7 0.0 copy-done.10
  4.7 1.2 %copy-done = f32[2,8,128,128]{3,2,1,0:T(8,128)S(1)} copy-done((f32[2,8,128,128]{3,2,1,0:T(8,128)S(1)}, f32[2,8,128,128]{3,2,1,0:T(8,128)}, u32[]{:S(2)}) %copy-start) | copy-done | bytes 1048600
  5.9 0.9 copy-done.2
  6.9 0.9 copy-done.3
  7.8 0.9 copy-done.4
  8.8 0.9 copy-done.5
  9.7 91.7 %decode_step.1 = (bf16[32,64]{1,0:T(8,128)(2,1)S(1)}, f32[2,8,128,128]{3,2,1,0:T(8,128)S(1)}) custom-call(bf16[32,64]{1,0:T(8,128)(2,1)S(1)} %copy-done.6, f32[2,8,128,128]{3,2,1,0:T(8,128)S(1)} %copy-done, f32[1,128]{1,0:T(1,128)S(1)} %bitcast.12, bf16[128,1024]{1,0:T(8,128)(2,1)S(1)} %copy-done.2, bf16[128,1024]{1,0:T(8,128)(2,1)S(1)} %copy-done.3, ...), custom_call_target="tpu_custom_call" | custom-call | tf_op jit(solution)/shard_map/decode_step/pallas_call | solution.py:369
  101.4 0.6 copy.21
  102.0 1.0 copy.22
  (6 shorter events, 0.0 us)
Async XLA Ops:
  0.6 1.3 %copy-start.11 = (bf16[2048,176]{0,1:T(8,128)(2,1)S(1)}, bf16[2048,176]{0,1:T(8,128)(2,1)}, u32[]{:S(2)}) copy-start(bf16[2048,176]{0,1:T(8,128)(2,1)} %param.25) | copy-start | bytes 2162692
  2.5 1.6 %copy-start.1 = (bf16[176,2048]{1,0:T(8,128)(2,1)S(1)}, bf16[176,2048]{1,0:T(8,128)(2,1)}, u32[]{:S(2)}) copy-start(bf16[176,2048]{1,0:T(8,128)(2,1)} %w_down.1) | copy-start | bytes 2162692
  2.5 1.6 %copy-start.6 = (bf16[32,64]{1,0:T(8,128)(2,1)S(1)}, bf16[32,64]{1,0:T(8,128)(2,1)}, u32[]{:S(2)}) copy-start(bf16[32,64]{1,0:T(8,128)(2,1)} %tokens.1) | copy-start | bytes 12292
  2.5 1.6 %copy-start.7 = (f32[2048]{0:T(1024)S(1)}, f32[2048]{0:T(1024)}, u32[]{:S(2)}) copy-start(f32[2048]{0:T(1024)} %param.24) | copy-start | bytes 24580
  2.5 1.6 %copy-start.8 = (f32[1024]{0:T(1024)S(1)}, f32[1024]{0:T(1024)}, u32[]{:S(2)}) copy-start(f32[1024]{0:T(1024)} %param.21) | copy-start | bytes 12292
  4.0 0.7 copy-start.9
  4.0 0.7 copy-start.10
  4.7 1.2 %copy-start = (f32[2,8,128,128]{3,2,1,0:T(8,128)S(1)}, f32[2,8,128,128]{3,2,1,0:T(8,128)}, u32[]{:S(2)}) copy-start(f32[2,8,128,128]{3,2,1,0:T(8,128)} %past_state.1) | copy-start | bytes 3145732
  5.9 0.9 copy-start.2
  6.9 0.9 copy-start.3
  7.8 0.9 copy-start.4
  8.8 0.9 copy-start.5

commit v2 on v1

--- a/solution.py
+++ b/solution.py
@@ -15,6 +15,10 @@
 
 def dot(a, b):
     return jnp.dot(a, b, preferred_element_type=F32)
+
+
+def dot_t(a, b):
+    return lax.dot_general(a, b, (((1,), (1,)), ((), ())), preferred_element_type=F32)
 
 
 def packed(x):
@@ -60,6 +64,7 @@
     mix,
     part_out,
     part_in,
+    mid_own,
     mid,
     wide_out,
     wide_in,
@@ -84,7 +89,7 @@
     other = 1 - c
     rows, feats = tokens.shape
     seqs, heads_local, dk, dv = past_state.shape
-    units = w_gate.shape[3]
+    units = w_gate.shape[0]
     group = heads_local * seqs
     half_rows = rows // 2
     width = kv * tp * feats
@@ -124,9 +129,9 @@
     half_of = pl.ds(pl.multiple_of(c * half_cols, half_cols), half_cols)
     half_of_other = pl.ds(pl.multiple_of(other * half_cols, half_cols), half_cols)
     weight_copies = [
-        local(w_out.at[c], out_w.at[0], 5),
-        local(w_gate.at[:, c], mlp_w.at[0], 6),
-        local(w_up.at[:, c], mlp_w.at[2], 7),
+        local(w_out.at[:, half_of], out_w.at[0], 5),
+        local(w_gate.at[:, half_of], mlp_w.at[0], 6),
+        local(w_up.at[:, half_of], mlp_w.at[2], 7),
         local(w_down.at[:, half_of], down_w.at[0], 8),
     ]
 
@@ -173,9 +178,9 @@
         sq[d].start()
         rs[d].start()
     swaps = [
-        remote(w_out.at[other], out_w.at[1], pair_send.at[1], pair_recv.at[1], z, other),
-        remote(w_gate.at[:, other], mlp_w.at[1], pair_send.at[2], pair_recv.at[2], z, other),
-        remote(w_up.at[:, other], mlp_w.at[3], pair_send.at[3], pair_recv.at[3], z, other),
+        remote(w_out.at[:, half_of_other], out_w.at[1], pair_send.at[1], pair_recv.at[1], z, other),
+        remote(w_gate.at[:, half_of_other], mlp_w.at[1], pair_send.at[2], pair_recv.at[2], z, other),
+        remote(w_up.at[:, half_of_other], mlp_w.at[3], pair_send.at[3], pair_recv.at[3], z, other),
         remote(w_down.at[:, half_of_other], down_w.at[1], pair_send.at[4], pair_recv.at[4], z, other),
     ]
     for s in swaps:
@@ -230,36 +235,50 @@
         ag[d].wait_recv()
     by_head = dot(gather, mix[...].reshape(kv * group, dv)).astype(BF16)
     every = jnp.concatenate([by_head[h * rows : (h + 1) * rows] for h in range(heads_local)], axis=1)
-    part_out[...] = packed(dot(every, out_w[1]))
+    part_out[...] = packed(dot_t(every, out_w[1]))
     part = remote(part_out, part_in, pair_send.at[5], pair_recv.at[5], z, other)
     part.start()
-    kept = packed(dot(every, out_w[0])) + packed(own)
+    kept = packed(dot_t(every, out_w[0])) + packed(own)
     part.wait_recv()
     middle = (kept + part_in[...]).astype(BF16)
-    mid[z] = middle
+    mid_own[...] = middle
+    half = z // half_kv
+    half_z = lax.rem(z, half_kv)
+    kept_here = half == c
     am = {}
     for d in far_first:
-        am[d] = remote(mid.at[z], mid.at[z], mid_send.at[d], mid_recv.at[d], peer(d), c)
+        am[d] = remote(mid_own, mid.at[half_z, c], mid_send.at[d], mid_recv.at[half_z, c], peer(d), half)
         am[d].start()
-
-    gain = mlp_gain[...]
-    gain_swapped = halves_swapped(gain)
-    first = c == 0
-    gain_low = jnp.where(first, gain, gain_swapped)
-    gain_high = jnp.where(first, gain_swapped, gain)
+    am_pair = remote(mid_own, mid.at[half_z, c], mid_send.at[0], mid_recv.at[half_z, c], z, half)
+
+    @pl.when(kept_here)
+    def _():
+        mid[half_z, c] = middle
+
+    @pl.when(jnp.logical_not(kept_here))
+    def _():
+        am_pair.start()
+
+    gain = mlp_gain[pl.ds(pl.multiple_of(c * half_kv, half_kv), half_kv), :]
     for w in weight_copies[1:]:
         w.wait()
     for s in swaps[1:]:
         s.wait_recv()
-    for d in near_first:
-        am[d].wait_recv()
+    for i in range(half_kv):
+        for from_c in range(tp):
+            from_self = jnp.logical_and(c * half_kv + i == z, c == from_c)
+
+            @pl.when(jnp.logical_not(from_self))
+            def _(i=i, from_c=from_c):
+                remote(mid_own, mid.at[i, from_c], mid_send.at[0], mid_recv.at[i, from_c], z, other).wait_recv()
+
     tops, bottoms = [], []
     squares = jnp.zeros((half_rows, tp * feats), F32)
-    for i in range(kv // 2):
-        a = mid[2 * i].astype(F32)
-        b = mid[2 * i + 1].astype(F32)
+    for i in range(half_kv):
+        a = mid[i, 0].astype(F32)
+        b = mid[i, 1].astype(F32)
         squares = squares + a * a + b * b
-        g = jnp.where(low, gain_low[2 * i : 2 * i + 1], gain_high[2 * i + 1 : 2 * i + 2])
+        g = gain[i : i + 1]
         tops.append((jnp.where(low, a, halves_swapped(b)) * g).astype(BF16))
         bottoms.append((jnp.where(low, halves_swapped(a), b) * g).astype(BF16))
     features = jnp.concatenate(
@@ -270,7 +289,7 @@
     sq_mid = jnp.concatenate([sq_top, sq_bottom], axis=0)
     sums = []
     for i in range(4):
-        sums.append(dot(features, mlp_w[i].reshape(kv * feats, units)))
+        sums.append(dot_t(features, mlp_w[i]))
         wide_out[i, :, pl.ds(0, units)] = sums[i]
     wide_out[4, :, :] = jnp.broadcast_to(sq_mid, wide_out.shape[1:])
     wide = remote(wide_out, wide_in, pair_send.at[6], pair_recv.at[6], z, other)
@@ -329,6 +348,11 @@
         sq[d].wait_send()
         ag[d].wait_send()
         am[d].wait_send()
+
+    @pl.when(jnp.logical_not(kept_here))
+    def _():
+        am_pair.wait_send()
+
     for copy, to_self, n in sends:
 
         @pl.when(jnp.logical_not(to_self))
@@ -394,8 +418,8 @@
             pltpu.VMEM((rows, feats), BF16),
             pltpu.VMEM((4, *w_query.shape), BF16),
             pltpu.VMEM(past_state.shape, F32),
-            pltpu.VMEM((2, channels, feats), BF16),
-            pltpu.VMEM((4, kv, feats, units), BF16),
+            pltpu.VMEM((2, feats, channels), BF16),
+            pltpu.VMEM((4, units, half_cols), BF16),
             pltpu.VMEM((2, units, half_cols), BF16),
             pltpu.VMEM((group, dk), F32),
             pltpu.VMEM((group, dv), F32),
@@ -406,7 +430,8 @@
             pltpu.VMEM((kv, group, dv), BF16),
             pltpu.VMEM((rows // 2, 2 * feats), F32),
             pltpu.VMEM((rows // 2, 2 * feats), F32),
-            pltpu.VMEM((kv, rows // 2, 2 * feats), BF16),
+            pltpu.VMEM((rows // 2, 2 * feats), BF16),
+            pltpu.VMEM((kv // tp, tp, rows // 2, 2 * feats), BF16),
             pltpu.VMEM((5, rows, wide), F32),
             pltpu.VMEM((5, rows, wide), F32),
             pltpu.VMEM((kv, rows // 2, 2 * feats), BF16),
@@ -421,12 +446,12 @@
             dma((kv,)),
             dma((kv,)),
             dma((kv,)),
-            dma((kv,)),
+            dma((kv // tp, tp)),
             dma((kv,)),
             dma((kv,)),
         ],
         compiler_params=pltpu.CompilerParams(
-            collective_id=0, has_side_effects=True, vmem_limit_bytes=32 * 1024 * 1024
+            collective_id=0, has_side_effects=True, vmem_limit_bytes=67043328
         ),
     )(
         tokens,
@@ -438,10 +463,10 @@
         w_gate_out,
         floor_logits.reshape(heads_local, dk),
         head_gain.reshape(1, -1),
-        w_out.reshape(tp, channels, feats),
+        w_out.T,
         mlp_gain.reshape(kv, tp * feats),
-        w_gate.reshape(kv, tp, feats, units),
-        w_up.reshape(kv, tp, feats, units),
+        w_gate.T,
+        w_up.T,
         w_down,
     )
 

time: 104 us -> 97.4 us (0.937)
  local copies, waits for them, and re-layouts: 10.5 us -> 3.59 us
  Pallas kernels: 91.7 us -> 92.9 us
    unnamed x29 -> x2, local copies, waits for them, and re-layouts: 10.5 us -> 3.59 us
    pallas_call x1, Pallas kernels: 91.7 us -> 92.9 us  [body(): pl.pallas_call(functools.partial(kernel, kv, tp), name='decode_step', out...]
where the time goes in v2:
time: 97.4 us; the launch traced here: 97.1 us
  Pallas kernels  92.9 us (95%)
  local copies, waits for them, and re-layouts  3.59 us (4%)
    pallas_call x1, Pallas kernels, body(): pl.pallas_call(functools.partial(kernel, kv, tp), name='decode_step', out...  92.9 us
    unnamed x2, local copies, waits for them, and re-layouts  3.59 us

profile of v2, /device:TPU:65, one launch (start us, length us, event | category | flops | bytes accessed | tf_op | source)
XLA Modules:
  0.0 97.1 jit_solution(17825866132125378455)
XLA Ops:
  0.6 92.9 %decode_step.1 = (bf16[32,64]{1,0:T(8,128)(2,1)}, f32[2,8,128,128]{3,2,1,0:T(8,128)}) custom-call(bf16[32,64]{1,0:T(8,128)(2,1)} %tokens.1, f32[2,8,128,128]{3,2,1,0:T(8,128)} %past_state.1, f32[1,128]{1,0:T(1,128)} %bitcast.12, bf16[128,1024]{1,0:T(8,128)(2,1)} %w_query.1, bf16[128,1024]{1,0:T(8,128)(2,1)} %w_forget.1, bf16[128,1024]{1,0:T(8,128)(2,1)} %w_value.1, ...), custom_call_target="tpu_custom_call" | custom-call | tf_op jit(solution)/shard_map/decode_step/pallas_call | solution.py:393
  93.5 1.3 %copy.18 = bf16[32,64]{1,0:T(8,128)(2,1)} copy(bf16[32,64]{1,0:T(8,128)(2,1)} %get-tuple-element.4) | data formatting | bytes 8192
  94.8 2.3 %copy.19 = f32[2,8,128,128]{3,2,1,0:T(8,128)} copy(f32[2,8,128,128]{3,2,1,0:T(8,128)} %get-tuple-element.5) | data formatting | bytes 2097152

commit v3 on v2

--- a/solution.py
+++ b/solution.py
@@ -9,6 +9,7 @@
 
 MESH = pl.DeviceIdType.MESH
 EPS = 1e-06
+VMEM_BYTES = 65_600_000
 F32 = jnp.float32
 BF16 = jnp.bfloat16
 
@@ -33,22 +34,28 @@
 def kernel(
     kv,
     tp,
-    tokens,
+    tokens_hbm,
     past_state,
-    mix_gain,
+    mix_gain_hbm,
     w_query,
     w_forget,
     w_value,
     w_gate_out,
-    floor_logits,
-    head_gain,
+    floor_hbm,
+    head_gain_hbm,
     w_out,
-    mlp_gain,
+    mlp_gain_hbm,
     w_gate,
     w_up,
     w_down,
     result,
-    new_state,
+    forget_out,
+    value_out,
+    tokens,
+    mix_gain,
+    floor_logits,
+    head_gain,
+    mlp_gain,
     tok_other,
     proj_w,
     state,
@@ -83,6 +90,8 @@
     mid_recv,
     term_send,
     term_recv,
+    pair_in,
+    ready,
 ):
     z = lax.axis_index("kv")
     c = lax.axis_index("tp")
@@ -114,18 +123,33 @@
     def peer(d):
         return lax.rem(z + d, kv)
 
+    def place(w):
+        return lax.rem(w + kv - 1, kv)
+
+    order = [*range(1, kv), 0]
     far_first = sorted(range(1, kv), key=lambda d: -min(d, kv - d))
     near_first = far_first[::-1]
 
     barrier = pltpu.get_barrier_semaphore()
-    for d in far_first:
-        pl.semaphore_signal(barrier, inc=1, device_id={"kv": peer(d), "tp": c}, device_id_type=MESH)
-    pl.semaphore_signal(barrier, inc=1, device_id={"kv": z, "tp": other}, device_id_type=MESH)
-
+
+    def signal(sem, to_z, to_c):
+        pl.semaphore_signal(sem, inc=1, device_id={"kv": to_z, "tp": to_c}, device_id_type=MESH)
+
+    @pl.when(c == 1)
+    def _():
+        signal(barrier, z, 0)
+
+    tokens_copy = local(tokens_hbm, tokens, 9)
+    gain_copy = local(mix_gain_hbm, mix_gain, 10)
     proj_copies = [
         local(w, proj_w.at[i], i) for i, w in enumerate((w_query, w_forget, w_value, w_gate_out))
     ]
     state_copy = local(past_state, state, 4)
+    small_copies = [
+        local(floor_hbm, floor_logits, 11),
+        local(head_gain_hbm, head_gain, 12),
+        local(mlp_gain_hbm, mlp_gain, 13),
+    ]
     half_of = pl.ds(pl.multiple_of(c * half_cols, half_cols), half_cols)
     half_of_other = pl.ds(pl.multiple_of(other * half_cols, half_cols), half_cols)
     weight_copies = [
@@ -135,6 +159,43 @@
         local(w_down.at[:, half_of], down_w.at[0], 8),
     ]
 
+    @pl.when(c == 0)
+    def _():
+        pl.semaphore_wait(barrier, 1)
+        signal(pair_in, z, 1)
+
+    @pl.when(c == 1)
+    def _():
+        pl.semaphore_wait(pair_in, 1)
+        for w in order:
+
+            @pl.when(place(z) < place(w))
+            def _(w=w):
+                signal(barrier, w, 1)
+
+    tokens_copy.wait()
+    tok = remote(tokens, tok_other, pair_send.at[0], pair_recv.at[0], z, other)
+    tok.start()
+
+    @pl.when(c == 1)
+    def _():
+        @pl.when(place(z) > 0)
+        def _():
+            pl.semaphore_wait(barrier, place(z))
+
+        signal(pair_in, z, 0)
+
+    @pl.when(c == 0)
+    def _():
+        pl.semaphore_wait(pair_in, 1)
+
+    for d in far_first:
+        to = peer(d)
+
+        @pl.when(place(to) < place(z))
+        def _(to=to):
+            signal(ready.at[z], to, c)
+
     r = lax.broadcasted_iota(jnp.int32, (kv * group, kv * group), 0)
     col = lax.broadcasted_iota(jnp.int32, (kv * group, kv * group), 1)
     s_of = lax.rem(r, seqs)
@@ -143,14 +204,6 @@
     to_heads = lax.rem(r // seqs, kv) * group + (r // (kv * seqs)) * seqs + s_of
     gather = jnp.where(col == to_heads, 1.0, 0.0).astype(BF16)
 
-    lower_in = jax.nn.sigmoid(floor_logits[...])
-    for h in range(heads_local):
-        floors[pl.ds(h * seqs, seqs), :] = jnp.broadcast_to(lower_in[h : h + 1], (seqs, dk))
-
-    pl.semaphore_wait(barrier, kv)
-
-    tok = remote(tokens, tok_other, pair_send.at[0], pair_recv.at[0], z, other)
-    tok.start()
     lane = lax.broadcasted_iota(jnp.int32, (1, tp * feats), 1)
     low = lane < feats
     own = tokens[...].astype(F32)
@@ -162,6 +215,7 @@
     block = jnp.where(mine, own_twice, got_twice)
     squares = jnp.sum(block * block, axis=1, keepdims=True)
     sq_out[...] = jnp.broadcast_to(squares, (rows, dk)).reshape(kv, seqs, dk)
+    gain_copy.wait()
     gained = (block * mix_gain[...]).astype(BF16)
     for i in range(4):
         proj_copies[i].wait()
@@ -170,13 +224,20 @@
         ordered = dot(spread, stack).astype(BF16)
         chunk_out[:, pl.ds(i * group, group), :] = ordered.reshape(kv, group, dk)
 
-    rs, sq = {}, {}
+    def send_chunk(to, start):
+        for copy in (
+            remote(sq_out.at[to], sq_in.at[z], sq_send.at[to], sq_recv.at[z], to, c),
+            remote(chunk_out.at[to], chunk_in.at[z], rs_send.at[to], rs_recv.at[z], to, c),
+        ):
+            copy.start() if start else copy.wait_send()
+
     for d in far_first:
         to = peer(d)
-        rs[d] = remote(chunk_out.at[to], chunk_in.at[d], rs_send.at[d], rs_recv.at[d], to, c)
-        sq[d] = remote(sq_out.at[to], sq_in.at[d], sq_send.at[d], sq_recv.at[d], to, c)
-        sq[d].start()
-        rs[d].start()
+
+        @pl.when(place(to) < place(z))
+        def _(to=to):
+            send_chunk(to, True)
+
     swaps = [
         remote(w_out.at[:, half_of_other], out_w.at[1], pair_send.at[1], pair_recv.at[1], z, other),
         remote(w_gate.at[:, half_of_other], mlp_w.at[1], pair_send.at[2], pair_recv.at[2], z, other),
@@ -186,13 +247,32 @@
     for s in swaps:
         s.start()
 
-    total_sq = sq_out[z]
-    total = chunk_out[z].astype(F32)
-    for d in near_first:
-        sq[d].wait_recv()
-        total_sq = total_sq + sq_in[d]
-        rs[d].wait_recv()
-        total = total + chunk_in[d].astype(F32)
+    sq_in[z] = sq_out[z]
+    chunk_in[z] = chunk_out[z]
+    for copy in small_copies:
+        copy.wait()
+    lower_in = jax.nn.sigmoid(floor_logits[...])
+    for h in range(heads_local):
+        floors[pl.ds(h * seqs, seqs), :] = jnp.broadcast_to(lower_in[h : h + 1], (seqs, dk))
+
+    for w in order:
+
+        @pl.when(place(z) < place(w))
+        def _(w=w):
+            pl.semaphore_wait(ready.at[w], 1)
+            send_chunk(w, True)
+
+    total_sq = jnp.zeros((seqs, dk), F32)
+    total = jnp.zeros((4 * group, dk), F32)
+    for w in order:
+
+        @pl.when(z != w)
+        def _(w=w):
+            remote(sq_out.at[w], sq_in.at[w], sq_send.at[w], sq_recv.at[w], w, c).wait_recv()
+            remote(chunk_out.at[w], chunk_in.at[w], rs_send.at[w], rs_recv.at[w], w, c).wait_recv()
+
+        total_sq = total_sq + sq_in[w]
+        total = total + chunk_in[w].astype(F32)
 
     scale_s = lax.rsqrt(total_sq / width + EPS)
     row_of = lax.broadcasted_iota(jnp.int32, (group, dk), 0)
@@ -216,10 +296,7 @@
             f_col = columns[:, i : i + 1]
             q_col = columns[:, group + i : group + i + 1]
             new = v_row + f_col * (state[s, h] - v_row)
-            state[s, h] = new
             heads[pl.ds(i, 1), :] = jnp.sum(new * q_col, axis=0, keepdims=True)
-    state_out = pltpu.make_async_copy(state, new_state, local_sem.at[4])
-    state_out.start()
 
     head_out = heads[...]
     normed = head_out * lax.rsqrt(jnp.mean(head_out * head_out, axis=1, keepdims=True) + EPS)
@@ -229,6 +306,11 @@
     for d in far_first:
         ag[d] = remote(mix.at[z], mix.at[z], mix_send.at[d], mix_recv.at[d], peer(d), c)
         ag[d].start()
+    for h in range(heads_local):
+        for s in range(seqs):
+            i = h * seqs + s
+            forget_out[s, pl.ds(h, 1), :] = forget[i : i + 1]
+            value_out[s, pl.ds(h, 1), :] = value[i : i + 1]
     weight_copies[0].wait()
     swaps[0].wait_recv()
     for d in near_first:
@@ -344,8 +426,7 @@
     for s in swaps:
         s.wait_send()
     for d in near_first:
-        rs[d].wait_send()
-        sq[d].wait_send()
+        send_chunk(peer(d), False)
         ag[d].wait_send()
         am[d].wait_send()
 
@@ -358,8 +439,6 @@
         @pl.when(jnp.logical_not(to_self))
         def _(copy=copy):
             copy.wait_send()
-
-    state_out.wait()
 
 
 def body(
@@ -388,33 +467,23 @@
     half_cols = w_down.shape[1] // tp
     wide = -(-units // 128) * 128
     in_vmem = pl.BlockSpec(memory_space=pltpu.VMEM)
-    anywhere = pl.BlockSpec(memory_space=pl.ANY)
     dma = pltpu.SemaphoreType.DMA
-    return pl.pallas_call(
+    result, forget, value = pl.pallas_call(
         functools.partial(kernel, kv, tp),
         name="decode_step",
         out_shape=(
             jax.ShapeDtypeStruct((rows, feats), BF16),
-            jax.ShapeDtypeStruct(past_state.shape, F32),
+            jax.ShapeDtypeStruct((seqs, heads_local, dk), F32),
+            jax.ShapeDtypeStruct((seqs, heads_local, dv), F32),
         ),
-        in_specs=[
-            in_vmem,
-            anywhere,
-            in_vmem,
-            anywhere,
-            anywhere,
-            anywhere,
-            anywhere,
-            in_vmem,
-            in_vmem,
-            anywhere,
-            in_vmem,
-            anywhere,
-            anywhere,
-            anywhere,
-        ],
-        out_specs=(in_vmem, anywhere),
+        in_specs=[pl.BlockSpec(memory_space=pltpu.HBM)] * 14,
+        out_specs=(in_vmem, in_vmem, in_vmem),
         scratch_shapes=[
+            pltpu.VMEM((rows, feats), BF16),
+            pltpu.VMEM((1, tp * feats), F32),
+            pltpu.VMEM((heads_local, dk), F32),
+            pltpu.VMEM((1, dv), F32),
+            pltpu.VMEM((kv, tp * feats), F32),
             pltpu.VMEM((rows, feats), BF16),
             pltpu.VMEM((4, *w_query.shape), BF16),
             pltpu.VMEM(past_state.shape, F32),
@@ -436,7 +505,7 @@
             pltpu.VMEM((5, rows, wide), F32),
             pltpu.VMEM((kv, rows // 2, 2 * feats), BF16),
             pltpu.VMEM((kv, rows // 2, 2 * feats), BF16),
-            dma((9,)),
+            dma((14,)),
             dma((7,)),
             dma((7,)),
             dma((kv,)),
@@ -449,9 +518,11 @@
             dma((kv // tp, tp)),
             dma((kv,)),
             dma((kv,)),
+            pltpu.SemaphoreType.REGULAR,
+            pltpu.SemaphoreType.REGULAR((kv,)),
         ],
         compiler_params=pltpu.CompilerParams(
-            collective_id=0, has_side_effects=True, vmem_limit_bytes=67043328
+            collective_id=0, has_side_effects=True, vmem_limit_bytes=VMEM_BYTES
         ),
     )(
         tokens,
@@ -469,6 +540,8 @@
         w_up.T,
         w_down,
     )
+    value = value[:, :, None, :]
+    return result, value + forget[..., None] * (past_state - value)
 
 
 def solution(mesh):

time: 97.4 us -> 85.5 us (0.88)
  Pallas kernels: 92.9 us -> 82 us
  local copies, waits for them, and re-layouts: 3.59 us -> 0.61 us
  other arithmetic: 0 us -> 2.03 us
    pallas_call x1, Pallas kernels: 92.9 us -> 82 us  [body(): pl.pallas_call(functools.partial(kernel, kv, tp), name='decode_step', out...]
    unnamed x2 -> x5, local copies, waits for them, and re-layouts: 3.59 us -> 0.61 us
    add x0 -> x1, other arithmetic: none -> 2.03 us  [body(): return (result, value + forget[..., None] * (past_state - value))]
where the time goes in v3:
time: 85.5 us; the launch traced here: 85.3 us
  Pallas kernels  82 us (96%)
  other arithmetic  2.03 us (2%)
    pallas_call x1, Pallas kernels, body(): pl.pallas_call(functools.partial(kernel, kv, tp), name='decode_step', out...  82 us
    add x1, other arithmetic, body(): return (result, value + forget[..., None] * (past_state - value))  2.03 us

profile of v3, /device:TPU:65, one launch (start us, length us, event | category | flops | bytes accessed | tf_op | source)
XLA Modules:
  0.0 85.3 jit_solution(192399201328092060)
XLA Ops:
  0.6 0.0 copy-start
  0.6 82.0 %decode_step.1 = (bf16[32,64]{1,0:T(8,128)(2,1)}, f32[2,8,128]{2,1,0:T(8,128)}, f32[2,8,128]{2,1,0:T(8,128)}) custom-call(bf16[32,64]{1,0:T(8,128)(2,1)} %tokens_hbm.1, f32[2,8,128,128]{3,2,1,0:T(8,128)} %past_state.1, f32[1,128]{1,0:T(1,128)} %bitcast.12, bf16[128,1024]{1,0:T(8,128)(2,1)} %w_query.1, bf16[128,1024]{1,0:T(8,128)(2,1)} %w_forget.1, ...), custom_call_target="tpu_custom_call" | custom-call | tf_op jit(solution)/shard_map/decode_step/pallas_call | solution.py:471
  82.7 0.0 copy-done
  82.7 0.0 copy-start.1
  82.7 2.0 %multiply_add_fusion = f32[2,8,128,128]{3,2,1,0:T(8,128)} fusion(f32[2,8,128,128]{3,2,1,0:T(8,128)S(1)} %copy-done, f32[2,8,128]{2,1,0:T(8,128)} %get-tuple-element.7, f32[2,8,128]{2,1,0:T(8,128)} %get-tuple-element.6), kind=kLoop, calls=%fused_computation | loop fusion | flops 786432 | bytes 2113536 | tf_op jit(solution)/shard_map/add | solution.py:544
  84.7 0.0 copy-done.1
  84.7 0.6 copy.17
Async XLA Ops:
  0.6 82.1 %copy-start = (f32[2,8,128,128]{3,2,1,0:T(8,128)S(1)}, f32[2,8,128,128]{3,2,1,0:T(8,128)}, u32[]{:S(2)}) copy-start(f32[2,8,128,128]{3,2,1,0:T(8,128)} %past_state.1) | copy-start | bytes 3145732
  82.7 2.0 %copy-start.1 = (bf16[32,64]{1,0:T(8,128)(2,1)S(1)}, bf16[32,64]{1,0:T(8,128)(2,1)}, u32[]{:S(2)}) copy-start(bf16[32,64]{1,0:T(8,128)(2,1)} %get-tuple-element.10) | copy-start | bytes 12292

commit v4 on v3

--- a/solution.py
+++ b/solution.py
@@ -9,7 +9,7 @@
 
 MESH = pl.DeviceIdType.MESH
 EPS = 1e-06
-VMEM_BYTES = 65_600_000
+VMEM_BYTES = 48 * 1024 * 1024
 F32 = jnp.float32
 BF16 = jnp.bfloat16
 
@@ -20,6 +20,10 @@
 
 def dot_t(a, b):
     return lax.dot_general(a, b, (((1,), (1,)), ((), ())), preferred_element_type=F32)
+
+
+def hbm(*arrays):
+    return [pltpu.with_memory_space_constraint(a, pltpu.HBM) for a in arrays]
 
 
 def packed(x):
@@ -124,9 +128,9 @@
         return lax.rem(z + d, kv)
 
     def place(w):
-        return lax.rem(w + kv - 1, kv)
-
-    order = [*range(1, kv), 0]
+        return jnp.where(w == 0, kv - 2, jnp.where(w == kv - 1, kv - 1, w - 1))
+
+    order = [*range(1, kv - 1), 0, kv - 1]
     far_first = sorted(range(1, kv), key=lambda d: -min(d, kv - d))
     near_first = far_first[::-1]
 
@@ -173,28 +177,28 @@
             def _(w=w):
                 signal(barrier, w, 1)
 
+    @pl.when(c == 1)
+    def _():
+        @pl.when(place(z) > 0)
+        def _():
+            pl.semaphore_wait(barrier, place(z))
+
+        signal(pair_in, z, 0)
+
+    @pl.when(c == 0)
+    def _():
+        pl.semaphore_wait(pair_in, 1)
+
+    for d in far_first:
+        to = peer(d)
+
+        @pl.when(place(to) < place(z))
+        def _(to=to):
+            signal(ready.at[z], to, c)
+
     tokens_copy.wait()
     tok = remote(tokens, tok_other, pair_send.at[0], pair_recv.at[0], z, other)
     tok.start()
-
-    @pl.when(c == 1)
-    def _():
-        @pl.when(place(z) > 0)
-        def _():
-            pl.semaphore_wait(barrier, place(z))
-
-        signal(pair_in, z, 0)
-
-    @pl.when(c == 0)
-    def _():
-        pl.semaphore_wait(pair_in, 1)
-
-    for d in far_first:
-        to = peer(d)
-
-        @pl.when(place(to) < place(z))
-        def _(to=to):
-            signal(ready.at[z], to, c)
 
     r = lax.broadcasted_iota(jnp.int32, (kv * group, kv * group), 0)
     col = lax.broadcasted_iota(jnp.int32, (kv * group, kv * group), 1)
@@ -217,26 +221,42 @@
     sq_out[...] = jnp.broadcast_to(squares, (rows, dk)).reshape(kv, seqs, dk)
     gain_copy.wait()
     gained = (block * mix_gain[...]).astype(BF16)
-    for i in range(4):
-        proj_copies[i].wait()
-        product = dot(gained, proj_w[i]).astype(BF16)
-        stack = jnp.concatenate([product[:, h * dk : (h + 1) * dk] for h in range(heads_local)], axis=0)
-        ordered = dot(spread, stack).astype(BF16)
-        chunk_out[:, pl.ds(i * group, group), :] = ordered.reshape(kv, group, dk)
-
-    def send_chunk(to, start):
-        for copy in (
-            remote(sq_out.at[to], sq_in.at[z], sq_send.at[to], sq_recv.at[z], to, c),
-            remote(chunk_out.at[to], chunk_in.at[z], rs_send.at[to], rs_recv.at[z], to, c),
-        ):
-            copy.start() if start else copy.wait_send()
+    def sq_copy(to):
+        return remote(sq_out.at[to], sq_in.at[z], sq_send.at[to], sq_recv.at[z], to, c)
+
+    def chunk_copy(to):
+        return remote(chunk_out.at[to], chunk_in.at[z], rs_send.at[to], rs_recv.at[z], to, c)
 
     for d in far_first:
         to = peer(d)
 
         @pl.when(place(to) < place(z))
         def _(to=to):
-            send_chunk(to, True)
+            sq_copy(to).start()
+
+    for copy in proj_copies:
+        copy.wait()
+    products = [dot(gained, proj_w[i]).astype(BF16) for i in range(4)]
+    for i in (0, 2):
+        stack = jnp.concatenate(
+            [
+                jnp.concatenate([p[:, h * dk : (h + 1) * dk] for p in products[i : i + 2]], axis=1)
+                for h in range(heads_local)
+            ],
+            axis=0,
+        )
+        ordered = dot(spread, stack).astype(BF16)
+        for j in range(2):
+            chunk_out[:, pl.ds((i + j) * group, group), :] = ordered[:, j * dk : (j + 1) * dk].reshape(
+                kv, group, dk
+            )
+
+    for d in far_first:
+        to = peer(d)
+
+        @pl.when(place(to) < place(z))
+        def _(to=to):
+            chunk_copy(to).start()
 
     swaps = [
         remote(w_out.at[:, half_of_other], out_w.at[1], pair_send.at[1], pair_recv.at[1], z, other),
@@ -260,7 +280,8 @@
         @pl.when(place(z) < place(w))
         def _(w=w):
             pl.semaphore_wait(ready.at[w], 1)
-            send_chunk(w, True)
+            sq_copy(w).start()
+            chunk_copy(w).start()
 
     total_sq = jnp.zeros((seqs, dk), F32)
     total = jnp.zeros((4 * group, dk), F32)
@@ -306,6 +327,10 @@
     for d in far_first:
         ag[d] = remote(mix.at[z], mix.at[z], mix_send.at[d], mix_recv.at[d], peer(d), c)
         ag[d].start()
+    tok.wait_send()
+    for d in far_first:
+        sq_copy(peer(d)).wait_send()
+        chunk_copy(peer(d)).wait_send()
     for h in range(heads_local):
         for s in range(seqs):
             i = h * seqs + s
@@ -341,6 +366,11 @@
     def _():
         am_pair.start()
 
+    part.wait_send()
+    for d in far_first:
+        ag[d].wait_send()
+    for copy in swaps:
+        copy.wait_send()
     gain = mlp_gain[pl.ds(pl.multiple_of(c * half_kv, half_kv), half_kv), :]
     for w in weight_copies[1:]:
         w.wait()
@@ -369,14 +399,18 @@
     sq_top = jnp.sum(jnp.where(low, squares, 0.0), axis=1, keepdims=True)
     sq_bottom = jnp.sum(jnp.where(low, 0.0, squares), axis=1, keepdims=True)
     sq_mid = jnp.concatenate([sq_top, sq_bottom], axis=0)
+    wide_out[4, :, :] = jnp.broadcast_to(sq_mid, wide_out.shape[1:])
+    wides = [
+        remote(wide_out.at[i], wide_in.at[i], pair_send.at[6 + i], pair_recv.at[6 + i], z, other) for i in range(5)
+    ]
+    wides[4].start()
     sums = []
     for i in range(4):
         sums.append(dot_t(features, mlp_w[i]))
         wide_out[i, :, pl.ds(0, units)] = sums[i]
-    wide_out[4, :, :] = jnp.broadcast_to(sq_mid, wide_out.shape[1:])
-    wide = remote(wide_out, wide_in, pair_send.at[6], pair_recv.at[6], z, other)
-    wide.start()
-    wide.wait_recv()
+        wides[i].start()
+    for copy in wides:
+        copy.wait_recv()
     mlp_scale = lax.rsqrt((sq_mid + wide_in[4, :, 0:1]) / width + EPS)
     terms = None
     for i in range(2):
@@ -409,6 +443,15 @@
             def _(n=n):
                 terms_in[z] = terms_out[n]
 
+    for copy in wides:
+        copy.wait_send()
+    for d in far_first:
+        am[d].wait_send()
+
+    @pl.when(jnp.logical_not(kept_here))
+    def _():
+        am_pair.wait_send()
+
     for i in range(kv):
         from_self = jnp.logical_and(i == z, c == z // half_kv)
 
@@ -419,20 +462,6 @@
     summed = middle.astype(F32) + jnp.sum(terms_in[...].astype(F32), axis=0)
     result[pl.ds(0, half_rows), :] = summed[:, :feats].astype(BF16)
     result[pl.ds(half_rows, half_rows), :] = summed[:, feats:].astype(BF16)
-
-    tok.wait_send()
-    part.wait_send()
-    wide.wait_send()
-    for s in swaps:
-        s.wait_send()
-    for d in near_first:
-        send_chunk(peer(d), False)
-        ag[d].wait_send()
-        am[d].wait_send()
-
-    @pl.when(jnp.logical_not(kept_here))
-    def _():
-        am_pair.wait_send()
 
     for copy, to_self, n in sends:
 
@@ -506,8 +535,8 @@
             pltpu.VMEM((kv, rows // 2, 2 * feats), BF16),
             pltpu.VMEM((kv, rows // 2, 2 * feats), BF16),
             dma((14,)),
-            dma((7,)),
-            dma((7,)),
+            dma((11,)),
+            dma((11,)),
             dma((kv,)),
             dma((kv,)),
             dma((kv,)),
@@ -524,7 +553,7 @@
         compiler_params=pltpu.CompilerParams(
             collective_id=0, has_side_effects=True, vmem_limit_bytes=VMEM_BYTES
         ),
-    )(
+    )(*hbm(
         tokens,
         past_state,
         mix_gain.reshape(1, -1),
@@ -539,7 +568,7 @@
         w_gate.T,
         w_up.T,
         w_down,
-    )
+    ))
     value = value[:, :, None, :]
     return result, value + forget[..., None] * (past_state - value)
 

time: 85.5 us -> 86.5 us (1.012)
  Pallas kernels: 82 us -> 83.8 us
    pallas_call x1, Pallas kernels: 82 us -> 83.8 us  [body(): pl.pallas_call(functools.partial(kernel, kv, tp), name='decode_step', out...]
where the time goes in v4:
time: 86.5 us; the launch traced here: 86.4 us
  Pallas kernels  83.8 us (97%)
  other arithmetic  1.31 us (2%)
    pallas_call x1, Pallas kernels, body(): pl.pallas_call(functools.partial(kernel, kv, tp), name='decode_step', out...  83.8 us

profile of v4, /device:TPU:65, one launch (start us, length us, event | category | flops | bytes accessed | tf_op | source)
XLA Modules:
  0.0 86.4 jit_solution(16987589591856851438)
XLA Ops:
  0.6 0.0 copy-start
  0.6 83.8 %decode_step.1 = (bf16[32,64]{1,0:T(8,128)(2,1)S(1)}, f32[2,8,128]{2,1,0:T(8,128)S(1)}, f32[2,8,128]{2,1,0:T(8,128)S(1)}) custom-call(bf16[32,64]{1,0:T(8,128)(2,1)} %tokens_hbm.1, f32[2,8,128,128]{3,2,1,0:T(8,128)} %past_state.1, f32[1,128]{1,0:T(1,128)} %bitcast.12, bf16[128,1024]{1,0:T(8,128)(2,1)} %w_query.1, bf16[128,1024]{1,0:T(8,128)(2,1)} %w_forget.1, ...), custom_call_target="tpu_custom_call" | custom-call | tf_op jit(solution)/shard_map/decode_step/pallas_call | solution.py:500
  84.5 0.0 copy-done
  84.5 1.3 %multiply_add_fusion = f32[2,8,128,128]{3,2,1,0:T(8,128)} fusion(f32[2,8,128,128]{3,2,1,0:T(8,128)S(1)} %copy-done, f32[2,8,128]{2,1,0:T(8,128)S(1)} %get-tuple-element.7, f32[2,8,128]{2,1,0:T(8,128)S(1)} %get-tuple-element.6), kind=kLoop, calls=%fused_computation | loop fusion | flops 786432 | bytes 2113536 | tf_op jit(solution)/shard_map/add | solution.py:573
  85.8 0.6 copy.17
Async XLA Ops:
  0.6 83.8 %copy-start = (f32[2,8,128,128]{3,2,1,0:T(8,128)S(1)}, f32[2,8,128,128]{3,2,1,0:T(8,128)}, u32[]{:S(2)}) copy-start(f32[2,8,128,128]{3,2,1,0:T(8,128)} %past_state.1) | copy-start | bytes 3145732

commit v5 on v4

--- a/solution.py
+++ b/solution.py
@@ -60,6 +60,7 @@
     floor_logits,
     head_gain,
     mlp_gain,
+    tok_own,
     tok_other,
     proj_w,
     state,
@@ -72,6 +73,11 @@
     chunk_in,
     sq_out,
     sq_in,
+    total,
+    relay_in,
+    relay_sq_in,
+    relayed_out,
+    relayed_in,
     mix,
     part_out,
     part_in,
@@ -94,6 +100,10 @@
     mid_recv,
     term_send,
     term_recv,
+    relay_recv,
+    relay_sq_recv,
+    relayed_send,
+    relayed_recv,
     pair_in,
     ready,
 ):
@@ -131,8 +141,17 @@
         return jnp.where(w == 0, kv - 2, jnp.where(w == kv - 1, kv - 1, w - 1))
 
     order = [*range(1, kv - 1), 0, kv - 1]
+    last = kv - 1
+    near_last = [w for w in range(kv - tp - 2, kv - 1)]
+    relays = {0: kv // 4, last: near_last[0] - 1}
+    behind = near_last[0] - 1
+    listeners = {0: [relays[0], *near_last], last: [relays[last], *near_last, 0]}
     far_first = sorted(range(1, kv), key=lambda d: -min(d, kv - d))
-    near_first = far_first[::-1]
+
+    def wait_all(buffer, count, sem, received=True):
+        part_of = buffer.at[pl.ds(0, count)]
+        copy = remote(part_of, part_of, sem, sem, z, other)
+        copy.wait_recv() if received else copy.wait_send()
 
     barrier = pltpu.get_barrier_semaphore()
 
@@ -143,24 +162,23 @@
     def _():
         signal(barrier, z, 0)
 
-    tokens_copy = local(tokens_hbm, tokens, 9)
-    gain_copy = local(mix_gain_hbm, mix_gain, 10)
-    proj_copies = [
-        local(w, proj_w.at[i], i) for i, w in enumerate((w_query, w_forget, w_value, w_gate_out))
-    ]
-    state_copy = local(past_state, state, 4)
+    tokens_copy = local(tokens_hbm, tokens, 2)
+    gain_copy = local(mix_gain_hbm, mix_gain, 3)
+    for i, w in enumerate((w_query, w_forget, w_value, w_gate_out)):
+        local(w, proj_w.at[i], 0)
+    state_copy = local(past_state, state, 1)
     small_copies = [
-        local(floor_hbm, floor_logits, 11),
-        local(head_gain_hbm, head_gain, 12),
-        local(mlp_gain_hbm, mlp_gain, 13),
+        local(floor_hbm, floor_logits, 4),
+        local(head_gain_hbm, head_gain, 5),
+        local(mlp_gain_hbm, mlp_gain, 6),
     ]
     half_of = pl.ds(pl.multiple_of(c * half_cols, half_cols), half_cols)
     half_of_other = pl.ds(pl.multiple_of(other * half_cols, half_cols), half_cols)
     weight_copies = [
-        local(w_out.at[:, half_of], out_w.at[0], 5),
-        local(w_gate.at[:, half_of], mlp_w.at[0], 6),
-        local(w_up.at[:, half_of], mlp_w.at[2], 7),
-        local(w_down.at[:, half_of], down_w.at[0], 8),
+        local(w_out.at[:, half_of], out_w.at[0], 7),
+        local(w_gate.at[:, half_of], mlp_w.at[0], 8),
+        local(w_up.at[:, half_of], mlp_w.at[1], 9),
+        local(w_down.at[:, half_of], down_w.at[0], 10),
     ]
 
     @pl.when(c == 0)
@@ -189,15 +207,25 @@
     def _():
         pl.semaphore_wait(pair_in, 1)
 
+    for special, told in listeners.items():
+
+        @pl.when(z == special)
+        def _(special=special, told=told):
+            for w in told:
+                if order.index(w) < order.index(special):
+                    signal(ready.at[special], w, c)
+
     for d in far_first:
         to = peer(d)
 
-        @pl.when(place(to) < place(z))
+        @pl.when((place(to) < place(z)) & (place(z) < kv - 2))
         def _(to=to):
             signal(ready.at[z], to, c)
 
     tokens_copy.wait()
-    tok = remote(tokens, tok_other, pair_send.at[0], pair_recv.at[0], z, other)
+    own = tokens[...].astype(F32)
+    tok_own[...] = packed(own).astype(BF16)
+    tok = remote(tok_own, tok_other, pair_send.at[0], pair_recv.at[0], z, other)
     tok.start()
 
     r = lax.broadcasted_iota(jnp.int32, (kv * group, kv * group), 0)
@@ -210,11 +238,13 @@
 
     lane = lax.broadcasted_iota(jnp.int32, (1, tp * feats), 1)
     low = lane < feats
-    own = tokens[...].astype(F32)
     own_twice = jnp.concatenate([own, own], axis=1)
     tok.wait_recv()
     got = tok_other[...].astype(F32)
-    got_twice = jnp.concatenate([got, got], axis=1)
+    got_swapped = halves_swapped(got)
+    got_twice = jnp.concatenate(
+        [jnp.where(low, got, got_swapped), jnp.where(low, got_swapped, got)], axis=0
+    )
     mine = lax.broadcasted_iota(jnp.int32, (rows, tp * feats), 1) // feats == c
     block = jnp.where(mine, own_twice, got_twice)
     squares = jnp.sum(block * block, axis=1, keepdims=True)
@@ -222,10 +252,20 @@
     gain_copy.wait()
     gained = (block * mix_gain[...]).astype(BF16)
     def sq_copy(to):
-        return remote(sq_out.at[to], sq_in.at[z], sq_send.at[to], sq_recv.at[z], to, c)
+        return remote(sq_out.at[to], sq_in.at[z], sq_send.at[0], sq_recv.at[0], to, c)
 
     def chunk_copy(to):
-        return remote(chunk_out.at[to], chunk_in.at[z], rs_send.at[to], rs_recv.at[z], to, c)
+        return remote(chunk_out.at[to], chunk_in.at[z], rs_send.at[0], rs_recv.at[0], to, c)
+
+    def sq_to_relay(special):
+        return remote(
+            sq_out.at[special], relay_sq_in.at[z - 1], sq_send.at[0], relay_sq_recv.at[0], relays[special], c
+        )
+
+    def chunk_to_relay(special):
+        return remote(
+            chunk_out.at[special], relay_in.at[z - 1], rs_send.at[0], relay_recv.at[0], relays[special], c
+        )
 
     for d in far_first:
         to = peer(d)
@@ -234,8 +274,13 @@
         def _(to=to):
             sq_copy(to).start()
 
-    for copy in proj_copies:
-        copy.wait()
+    for special, relay in relays.items():
+
+        @pl.when((z > relay) & (z <= behind))
+        def _(special=special):
+            sq_to_relay(special).start()
+
+    pltpu.make_async_copy(proj_w, proj_w, local_sem.at[0]).wait()
     products = [dot(gained, proj_w[i]).astype(BF16) for i in range(4)]
     for i in (0, 2):
         stack = jnp.concatenate(
@@ -258,9 +303,15 @@
         def _(to=to):
             chunk_copy(to).start()
 
+    for special, relay in relays.items():
+
+        @pl.when((z > relay) & (z <= behind))
+        def _(special=special):
+            chunk_to_relay(special).start()
+
     swaps = [
         remote(w_out.at[:, half_of_other], out_w.at[1], pair_send.at[1], pair_recv.at[1], z, other),
-        remote(w_gate.at[:, half_of_other], mlp_w.at[1], pair_send.at[2], pair_recv.at[2], z, other),
+        remote(w_gate.at[:, half_of_other], mlp_w.at[2], pair_send.at[2], pair_recv.at[2], z, other),
         remote(w_up.at[:, half_of_other], mlp_w.at[3], pair_send.at[3], pair_recv.at[3], z, other),
         remote(w_down.at[:, half_of_other], down_w.at[1], pair_send.at[4], pair_recv.at[4], z, other),
     ]
@@ -275,35 +326,83 @@
     for h in range(heads_local):
         floors[pl.ds(h * seqs, seqs), :] = jnp.broadcast_to(lower_in[h : h + 1], (seqs, dk))
 
-    for w in order:
+    for w in order[:-2]:
 
         @pl.when(place(z) < place(w))
         def _(w=w):
             pl.semaphore_wait(ready.at[w], 1)
             sq_copy(w).start()
             chunk_copy(w).start()
-
-    total_sq = jnp.zeros((seqs, dk), F32)
-    total = jnp.zeros((4 * group, dk), F32)
-    for w in order:
-
-        @pl.when(z != w)
-        def _(w=w):
-            remote(sq_out.at[w], sq_in.at[w], sq_send.at[w], sq_recv.at[w], w, c).wait_recv()
-            remote(chunk_out.at[w], chunk_in.at[w], rs_send.at[w], rs_recv.at[w], w, c).wait_recv()
-
-        total_sq = total_sq + sq_in[w]
-        total = total + chunk_in[w].astype(F32)
-
+            for special, relay in relays.items():
+                if relay == w:
+                    sq_to_relay(special).start()
+                    chunk_to_relay(special).start()
+
+    for special, relay in relays.items():
+        forward = remote(relayed_out, relayed_in, relayed_send.at[0], relayed_recv.at[0], special, c)
+
+        @pl.when(z == relay)
+        def _(special=special, forward=forward):
+            wait_all(relay_sq_in, behind - 1, relay_sq_recv.at[0])
+            wait_all(relay_in, behind - 1, relay_recv.at[0])
+            relay_sq_in[z - 1] = sq_out[special]
+            relay_in[z - 1] = chunk_out[special]
+            sums = relay_in[0].astype(F32)
+            squares = relay_sq_in[0]
+            for i in range(1, behind):
+                sums = sums + relay_in[i].astype(F32)
+                squares = squares + relay_sq_in[i]
+            relayed_out[pl.ds(0, 4 * group), :] = sums
+            relayed_out[pl.ds(4 * group, seqs), :] = squares
+            pl.semaphore_wait(ready.at[special], 1)
+            forward.start()
+
+        for w in listeners[special]:
+            if w != relay and order.index(w) < order.index(special):
+
+                @pl.when(z == w)
+                def _(special=special):
+                    pl.semaphore_wait(ready.at[special], 1)
+                    sq_copy(special).start()
+                    chunk_copy(special).start()
+
+    def add_up(slots):
+        sums = chunk_in[slots[0]].astype(F32)
+        squares = sq_in[slots[0]]
+        for w in slots[1:]:
+            sums = sums + chunk_in[w].astype(F32)
+            squares = squares + sq_in[w]
+        return sums, squares
+
+    is_special = (z == 0) | (z == last)
+
+    @pl.when(jnp.logical_not(is_special))
+    def _():
+        wait_all(sq_in, kv - 1, sq_recv.at[0])
+        wait_all(chunk_in, kv - 1, rs_recv.at[0])
+        sums, squares = add_up(order)
+        total[pl.ds(0, 4 * group), :] = sums
+        total[pl.ds(4 * group, seqs), :] = squares
+
+    @pl.when(is_special)
+    def _():
+        wait_all(sq_in, len(near_last) + 1, sq_recv.at[0])
+        wait_all(chunk_in, len(near_last) + 1, rs_recv.at[0])
+        sums, squares = add_up([*near_last, 0, last])
+        remote(relayed_out, relayed_in, relayed_send.at[0], relayed_recv.at[0], z, other).wait_recv()
+        total[pl.ds(0, 4 * group), :] = sums + relayed_in[pl.ds(0, 4 * group), :]
+        total[pl.ds(4 * group, seqs), :] = squares + relayed_in[pl.ds(4 * group, seqs), :]
+
+    total_sq = total[pl.ds(4 * group, seqs), :]
     scale_s = lax.rsqrt(total_sq / width + EPS)
     row_of = lax.broadcasted_iota(jnp.int32, (group, dk), 0)
     scale = jnp.broadcast_to(scale_s[0:1], (group, dk))
     for s in range(1, seqs):
         scale = jnp.where(lax.rem(row_of, seqs) == s, jnp.broadcast_to(scale_s[s : s + 1], (group, dk)), scale)
-    query = total[0:group] * scale
-    forget_pre = total[group : 2 * group] * scale
-    value = total[2 * group : 3 * group] * scale
-    gate_pre = total[3 * group : 4 * group] * scale
+    query = total[pl.ds(0, group), :] * scale
+    forget_pre = total[pl.ds(group, group), :] * scale
+    value = total[pl.ds(2 * group, group), :] * scale
+    gate_pre = total[pl.ds(3 * group, group), :] * scale
     lower = floors[...]
     forget = lower + (1.0 - lower) * jax.nn.sigmoid(forget_pre)
     activ = query * jax.nn.sigmoid(query)
@@ -323,14 +422,22 @@
     normed = head_out * lax.rsqrt(jnp.mean(head_out * head_out, axis=1, keepdims=True) + EPS)
     mixed = normed * head_gain[...] * (gate_pre * jax.nn.sigmoid(gate_pre))
     mix[z] = mixed.astype(BF16)
-    ag = {}
     for d in far_first:
-        ag[d] = remote(mix.at[z], mix.at[z], mix_send.at[d], mix_recv.at[d], peer(d), c)
-        ag[d].start()
+        remote(mix.at[z], mix.at[z], mix_send.at[0], mix_recv.at[0], peer(d), c).start()
     tok.wait_send()
-    for d in far_first:
-        sq_copy(peer(d)).wait_send()
-        chunk_copy(peer(d)).wait_send()
+    is_relay = (z == relays[0]) | (z == relays[last])
+
+    @pl.when(jnp.logical_not(is_relay))
+    def _():
+        wait_all(sq_in, kv - 1, sq_send.at[0], False)
+        wait_all(chunk_in, kv - 1, rs_send.at[0], False)
+
+    @pl.when(is_relay)
+    def _():
+        wait_all(sq_in, kv - 2, sq_send.at[0], False)
+        wait_all(chunk_in, kv - 2, rs_send.at[0], False)
+        remote(relayed_out, relayed_in, relayed_send.at[0], relayed_recv.at[0], z, other).wait_send()
+
     for h in range(heads_local):
         for s in range(seqs):
             i = h * seqs + s
@@ -338,8 +445,7 @@
             value_out[s, pl.ds(h, 1), :] = value[i : i + 1]
     weight_copies[0].wait()
     swaps[0].wait_recv()
-    for d in near_first:
-        ag[d].wait_recv()
+    wait_all(mix, kv - 1, mix_recv.at[0])
     by_head = dot(gather, mix[...].reshape(kv * group, dv)).astype(BF16)
     every = jnp.concatenate([by_head[h * rows : (h + 1) * rows] for h in range(heads_local)], axis=1)
     part_out[...] = packed(dot_t(every, out_w[1]))
@@ -352,23 +458,19 @@
     half = z // half_kv
     half_z = lax.rem(z, half_kv)
     kept_here = half == c
-    am = {}
     for d in far_first:
-        am[d] = remote(mid_own, mid.at[half_z, c], mid_send.at[d], mid_recv.at[half_z, c], peer(d), half)
-        am[d].start()
-    am_pair = remote(mid_own, mid.at[half_z, c], mid_send.at[0], mid_recv.at[half_z, c], z, half)
+        remote(mid_own, mid.at[half_z * tp + c], mid_send.at[0], mid_recv.at[0], peer(d), half).start()
 
     @pl.when(kept_here)
     def _():
-        mid[half_z, c] = middle
+        mid[half_z * tp + c] = middle
 
     @pl.when(jnp.logical_not(kept_here))
     def _():
-        am_pair.start()
+        remote(mid_own, mid.at[half_z * tp + c], mid_send.at[0], mid_recv.at[0], z, half).start()
 
     part.wait_send()
-    for d in far_first:
-        ag[d].wait_send()
+    wait_all(mix, kv - 1, mix_send.at[0], False)
     for copy in swaps:
         copy.wait_send()
     gain = mlp_gain[pl.ds(pl.multiple_of(c * half_kv, half_kv), half_kv), :]
@@ -376,19 +478,21 @@
         w.wait()
     for s in swaps[1:]:
         s.wait_recv()
-    for i in range(half_kv):
-        for from_c in range(tp):
-            from_self = jnp.logical_and(c * half_kv + i == z, c == from_c)
-
-            @pl.when(jnp.logical_not(from_self))
-            def _(i=i, from_c=from_c):
-                remote(mid_own, mid.at[i, from_c], mid_send.at[0], mid_recv.at[i, from_c], z, other).wait_recv()
-
+    def wait_others(buffer, sem, received=True):
+        @pl.when(kept_here)
+        def _():
+            wait_all(buffer, kv - 1, sem, received)
+
+        @pl.when(jnp.logical_not(kept_here))
+        def _():
+            wait_all(buffer, kv, sem, received)
+
+    wait_others(mid, mid_recv.at[0])
     tops, bottoms = [], []
     squares = jnp.zeros((half_rows, tp * feats), F32)
     for i in range(half_kv):
-        a = mid[i, 0].astype(F32)
-        b = mid[i, 1].astype(F32)
+        a = mid[tp * i].astype(F32)
+        b = mid[tp * i + 1].astype(F32)
         squares = squares + a * a + b * b
         g = gain[i : i + 1]
         tops.append((jnp.where(low, a, halves_swapped(b)) * g).astype(BF16))
@@ -401,7 +505,7 @@
     sq_mid = jnp.concatenate([sq_top, sq_bottom], axis=0)
     wide_out[4, :, :] = jnp.broadcast_to(sq_mid, wide_out.shape[1:])
     wides = [
-        remote(wide_out.at[i], wide_in.at[i], pair_send.at[6 + i], pair_recv.at[6 + i], z, other) for i in range(5)
+        remote(wide_out.at[i], wide_in.at[i], pair_send.at[6], pair_recv.at[6], z, other) for i in range(5)
     ]
     wides[4].start()
     sums = []
@@ -409,18 +513,16 @@
         sums.append(dot_t(features, mlp_w[i]))
         wide_out[i, :, pl.ds(0, units)] = sums[i]
         wides[i].start()
-    for copy in wides:
-        copy.wait_recv()
+    remote(wide_out, wide_in, pair_send.at[6], pair_recv.at[6], z, other).wait_recv()
     mlp_scale = lax.rsqrt((sq_mid + wide_in[4, :, 0:1]) / width + EPS)
     terms = None
     for i in range(2):
-        gate = (sums[i] + wide_in[1 - i, :, pl.ds(0, units)]) * mlp_scale
-        upward = (sums[2 + i] + wide_in[3 - i, :, pl.ds(0, units)]) * mlp_scale
+        gate = (sums[2 * i] + wide_in[2 - 2 * i, :, pl.ds(0, units)]) * mlp_scale
+        upward = (sums[2 * i + 1] + wide_in[3 - 2 * i, :, pl.ds(0, units)]) * mlp_scale
         hidden = (gate * jax.nn.sigmoid(gate) * upward).astype(BF16)
         term = dot(hidden, down_w[i])
         terms = term if terms is None else terms + term
 
-    sends = []
     for i in range(half_kv):
         at = slice(i * tp * feats, (i + 1) * tp * feats)
         top, bottom = terms[:half_rows, at], terms[half_rows:, at]
@@ -431,9 +533,8 @@
         ):
             n = 2 * i + to_c
             terms_out[n] = message.astype(BF16)
-            copy = remote(terms_out.at[n], terms_in.at[z], term_send.at[n], term_recv.at[z], to, to_c)
+            copy = remote(terms_out.at[n], terms_in.at[z], term_send.at[0], term_recv.at[0], to, to_c)
             to_self = jnp.logical_and(to == z, to_c == c)
-            sends.append((copy, to_self, n))
 
             @pl.when(jnp.logical_not(to_self))
             def _(copy=copy):
@@ -443,31 +544,14 @@
             def _(n=n):
                 terms_in[z] = terms_out[n]
 
-    for copy in wides:
-        copy.wait_send()
-    for d in far_first:
-        am[d].wait_send()
-
-    @pl.when(jnp.logical_not(kept_here))
-    def _():
-        am_pair.wait_send()
-
-    for i in range(kv):
-        from_self = jnp.logical_and(i == z, c == z // half_kv)
-
-        @pl.when(jnp.logical_not(from_self))
-        def _(i=i):
-            remote(terms_out.at[0], terms_in.at[i], term_send.at[0], term_recv.at[i], z, other).wait_recv()
-
+    remote(wide_out, wide_in, pair_send.at[6], pair_recv.at[6], z, other).wait_send()
+    wait_others(mid, mid_send.at[0], False)
+    wait_others(terms_in, term_recv.at[0])
     summed = middle.astype(F32) + jnp.sum(terms_in[...].astype(F32), axis=0)
     result[pl.ds(0, half_rows), :] = summed[:, :feats].astype(BF16)
     result[pl.ds(half_rows, half_rows), :] = summed[:, feats:].astype(BF16)
 
-    for copy, to_self, n in sends:
-
-        @pl.when(jnp.logical_not(to_self))
-        def _(copy=copy):
-            copy.wait_send()
+    wait_others(terms_in, term_send.at[0], False)
 
 
 def body(
@@ -513,7 +597,8 @@
             pltpu.VMEM((heads_local, dk), F32),
             pltpu.VMEM((1, dv), F32),
             pltpu.VMEM((kv, tp * feats), F32),
-            pltpu.VMEM((rows, feats), BF16),
+            pltpu.VMEM((rows // 2, 2 * feats), BF16),
+            pltpu.VMEM((rows // 2, 2 * feats), BF16),
             pltpu.VMEM((4, *w_query.shape), BF16),
             pltpu.VMEM(past_state.shape, F32),
             pltpu.VMEM((2, feats, channels), BF16),
@@ -525,28 +610,24 @@
             pltpu.VMEM((kv, 4 * group, dk), BF16),
             pltpu.VMEM((kv, seqs, dk), F32),
             pltpu.VMEM((kv, seqs, dk), F32),
+            pltpu.VMEM((4 * group + 8, dk), F32),
+            pltpu.VMEM((kv, 4 * group, dk), BF16),
+            pltpu.VMEM((kv, seqs, dk), F32),
+            pltpu.VMEM((4 * group + 8, dk), F32),
+            pltpu.VMEM((4 * group + 8, dk), F32),
             pltpu.VMEM((kv, group, dv), BF16),
             pltpu.VMEM((rows // 2, 2 * feats), F32),
             pltpu.VMEM((rows // 2, 2 * feats), F32),
             pltpu.VMEM((rows // 2, 2 * feats), BF16),
-            pltpu.VMEM((kv // tp, tp, rows // 2, 2 * feats), BF16),
+            pltpu.VMEM((kv, rows // 2, 2 * feats), BF16),
             pltpu.VMEM((5, rows, wide), F32),
             pltpu.VMEM((5, rows, wide), F32),
             pltpu.VMEM((kv, rows // 2, 2 * feats), BF16),
             pltpu.VMEM((kv, rows // 2, 2 * feats), BF16),
-            dma((14,)),
             dma((11,)),
-            dma((11,)),
-            dma((kv,)),
-            dma((kv,)),
-            dma((kv,)),
-            dma((kv,)),
-            dma((kv,)),
-            dma((kv,)),
-            dma((kv,)),
-            dma((kv // tp, tp)),
-            dma((kv,)),
-            dma((kv,)),
+            dma((7,)),
+            dma((7,)),
+            *[dma((1,))] * 14,
             pltpu.SemaphoreType.REGULAR,
             pltpu.SemaphoreType.REGULAR((kv,)),
         ],

time: 86.5 us -> 84.9 us (0.982)
  Pallas kernels: 83.8 us -> 82.1 us
    pallas_call x1, Pallas kernels: 83.8 us -> 82.1 us  [body(): pl.pallas_call(functools.partial(kernel, kv, tp), name='decode_step', out...]
where the time goes in v5:
time: 84.9 us; the launch traced here: 84.7 us
  Pallas kernels  82.1 us (97%)
  other arithmetic  1.31 us (2%)
    pallas_call x1, Pallas kernels, body(): pl.pallas_call(functools.partial(kernel, kv, tp), name='decode_step', out...  82.1 us

profile of v5, /device:TPU:65, one launch (start us, length us, event | category | flops | bytes accessed | tf_op | source)
XLA Modules:
  0.0 84.7 jit_solution(5317674996806069521)
XLA Ops:
  0.6 0.0 copy-start
  0.6 82.1 %decode_step.1 = (bf16[32,64]{1,0:T(8,128)(2,1)S(1)}, f32[2,8,128]{2,1,0:T(8,128)S(1)}, f32[2,8,128]{2,1,0:T(8,128)S(1)}) custom-call(bf16[32,64]{1,0:T(8,128)(2,1)} %tokens_hbm.1, f32[2,8,128,128]{3,2,1,0:T(8,128)} %past_state.1, f32[1,128]{1,0:T(1,128)} %bitcast.12, bf16[128,1024]{1,0:T(8,128)(2,1)} %w_query.1, bf16[128,1024]{1,0:T(8,128)(2,1)} %w_forget.1, ...), custom_call_target="tpu_custom_call" | custom-call | tf_op jit(solution)/shard_map/decode_step/pallas_call | solution.py:584
  82.8 0.0 copy-done
  82.8 1.3 %multiply_add_fusion = f32[2,8,128,128]{3,2,1,0:T(8,128)} fusion(f32[2,8,128,128]{3,2,1,0:T(8,128)S(1)} %copy-done, f32[2,8,128]{2,1,0:T(8,128)S(1)} %get-tuple-element.7, f32[2,8,128]{2,1,0:T(8,128)S(1)} %get-tuple-element.6), kind=kLoop, calls=%fused_computation | loop fusion | flops 786432 | bytes 2113536 | tf_op jit(solution)/shard_map/add | solution.py:654
  84.1 0.6 copy.17
Async XLA Ops:
  0.6 82.2 %copy-start = (f32[2,8,128,128]{3,2,1,0:T(8,128)S(1)}, f32[2,8,128,128]{3,2,1,0:T(8,128)}, u32[]{:S(2)}) copy-start(f32[2,8,128,128]{3,2,1,0:T(8,128)} %past_state.1) | copy-start | bytes 3145732

commit v6 on v5

--- a/solution.py
+++ b/solution.py
@@ -78,6 +78,7 @@
     relay_sq_in,
     relayed_out,
     relayed_in,
+    mix_own,
     mix,
     part_out,
     part_in,
@@ -153,6 +154,14 @@
         copy = remote(part_of, part_of, sem, sem, z, other)
         copy.wait_recv() if received else copy.wait_send()
 
+    first = pl.ds(0, 3 * group)
+    second = pl.ds(3 * group, group)
+
+    def wait_rows(buffer, count, at, sem, received=True):
+        part_of = buffer.at[pl.ds(0, count), at]
+        copy = remote(part_of, part_of, sem, sem, z, other)
+        copy.wait_recv() if received else copy.wait_send()
+
     barrier = pltpu.get_barrier_semaphore()
 
     def signal(sem, to_z, to_c):
@@ -175,7 +184,7 @@
     half_of = pl.ds(pl.multiple_of(c * half_cols, half_cols), half_cols)
     half_of_other = pl.ds(pl.multiple_of(other * half_cols, half_cols), half_cols)
     weight_copies = [
-        local(w_out.at[:, half_of], out_w.at[0], 7),
+        local(w_out.at[:, half_of_other], out_w.at[0], 7),
         local(w_gate.at[:, half_of], mlp_w.at[0], 8),
         local(w_up.at[:, half_of], mlp_w.at[1], 9),
         local(w_down.at[:, half_of], down_w.at[0], 10),
@@ -254,17 +263,25 @@
     def sq_copy(to):
         return remote(sq_out.at[to], sq_in.at[z], sq_send.at[0], sq_recv.at[0], to, c)
 
-    def chunk_copy(to):
-        return remote(chunk_out.at[to], chunk_in.at[z], rs_send.at[0], rs_recv.at[0], to, c)
+    def chunk_copy(to, at):
+        which = 0 if at is first else 1
+        return remote(
+            chunk_out.at[to, at], chunk_in.at[z, at], rs_send.at[which], rs_recv.at[which], to, c
+        )
 
     def sq_to_relay(special):
         return remote(
             sq_out.at[special], relay_sq_in.at[z - 1], sq_send.at[0], relay_sq_recv.at[0], relays[special], c
         )
 
-    def chunk_to_relay(special):
+    def chunk_to_relay(special, at):
         return remote(
-            chunk_out.at[special], relay_in.at[z - 1], rs_send.at[0], relay_recv.at[0], relays[special], c
+            chunk_out.at[special, at],
+            relay_in.at[z - 1, at],
+            rs_send.at[0 if at is first else 1],
+            relay_recv.at[0],
+            relays[special],
+            c,
         )
 
     for d in far_first:
@@ -296,27 +313,33 @@
                 kv, group, dk
             )
 
-    for d in far_first:
-        to = peer(d)
-
-        @pl.when(place(to) < place(z))
-        def _(to=to):
-            chunk_copy(to).start()
-
-    for special, relay in relays.items():
-
-        @pl.when((z > relay) & (z <= behind))
-        def _(special=special):
-            chunk_to_relay(special).start()
+    for at in (first, second):
+        for d in far_first:
+            to = peer(d)
+
+            @pl.when(place(to) < place(z))
+            def _(to=to, at=at):
+                chunk_copy(to, at).start()
+
+        for special, relay in relays.items():
+
+            @pl.when((z > relay) & (z <= behind))
+            def _(special=special, at=at):
+                chunk_to_relay(special, at).start()
 
     swaps = [
-        remote(w_out.at[:, half_of_other], out_w.at[1], pair_send.at[1], pair_recv.at[1], z, other),
+        remote(w_out.at[:, half_of], out_w.at[1], pair_send.at[1], pair_recv.at[1], z, other),
         remote(w_gate.at[:, half_of_other], mlp_w.at[2], pair_send.at[2], pair_recv.at[2], z, other),
         remote(w_up.at[:, half_of_other], mlp_w.at[3], pair_send.at[3], pair_recv.at[3], z, other),
         remote(w_down.at[:, half_of_other], down_w.at[1], pair_send.at[4], pair_recv.at[4], z, other),
     ]
-    for s in swaps:
-        s.start()
+    is_special = (z == 0) | (z == last)
+
+    @pl.when(jnp.logical_not(is_special))
+    def _():
+        for s in swaps:
+            s.start()
+
 
     sq_in[z] = sq_out[z]
     chunk_in[z] = chunk_out[z]
@@ -332,11 +355,13 @@
         def _(w=w):
             pl.semaphore_wait(ready.at[w], 1)
             sq_copy(w).start()
-            chunk_copy(w).start()
+            chunk_copy(w, first).start()
+            chunk_copy(w, second).start()
             for special, relay in relays.items():
                 if relay == w:
                     sq_to_relay(special).start()
-                    chunk_to_relay(special).start()
+                    chunk_to_relay(special, first).start()
+                    chunk_to_relay(special, second).start()
 
     for special, relay in relays.items():
         forward = remote(relayed_out, relayed_in, relayed_send.at[0], relayed_recv.at[0], special, c)
@@ -364,34 +389,40 @@
                 def _(special=special):
                     pl.semaphore_wait(ready.at[special], 1)
                     sq_copy(special).start()
-                    chunk_copy(special).start()
-
-    def add_up(slots):
-        sums = chunk_in[slots[0]].astype(F32)
+                    chunk_copy(special, first).start()
+                    chunk_copy(special, second).start()
+
+    def add_up(slots, at):
+        sums = chunk_in[slots[0], at].astype(F32)
+        for w in slots[1:]:
+            sums = sums + chunk_in[w, at].astype(F32)
+        return sums
+
+    def add_up_sq(slots):
         squares = sq_in[slots[0]]
         for w in slots[1:]:
-            sums = sums + chunk_in[w].astype(F32)
             squares = squares + sq_in[w]
-        return sums, squares
-
-    is_special = (z == 0) | (z == last)
+        return squares
+
+    direct = [*near_last, 0, last]
+    sq_rows = pl.ds(4 * group, seqs)
 
     @pl.when(jnp.logical_not(is_special))
     def _():
         wait_all(sq_in, kv - 1, sq_recv.at[0])
-        wait_all(chunk_in, kv - 1, rs_recv.at[0])
-        sums, squares = add_up(order)
-        total[pl.ds(0, 4 * group), :] = sums
-        total[pl.ds(4 * group, seqs), :] = squares
+        total[sq_rows, :] = add_up_sq(order)
+        wait_rows(chunk_in, kv - 1, first, rs_recv.at[0])
+        total[first, :] = add_up(order, first)
 
     @pl.when(is_special)
     def _():
-        wait_all(sq_in, len(near_last) + 1, sq_recv.at[0])
-        wait_all(chunk_in, len(near_last) + 1, rs_recv.at[0])
-        sums, squares = add_up([*near_last, 0, last])
+        wait_all(sq_in, len(direct) - 1, sq_recv.at[0])
+        wait_rows(chunk_in, len(direct) - 1, first, rs_recv.at[0])
         remote(relayed_out, relayed_in, relayed_send.at[0], relayed_recv.at[0], z, other).wait_recv()
-        total[pl.ds(0, 4 * group), :] = sums + relayed_in[pl.ds(0, 4 * group), :]
-        total[pl.ds(4 * group, seqs), :] = squares + relayed_in[pl.ds(4 * group, seqs), :]
+        total[first, :] = add_up(direct, first) + relayed_in[first, :]
+        total[sq_rows, :] = add_up_sq(direct) + relayed_in[sq_rows, :]
+        for s in swaps:
+            s.start()
 
     total_sq = total[pl.ds(4 * group, seqs), :]
     scale_s = lax.rsqrt(total_sq / width + EPS)
@@ -402,7 +433,6 @@
     query = total[pl.ds(0, group), :] * scale
     forget_pre = total[pl.ds(group, group), :] * scale
     value = total[pl.ds(2 * group, group), :] * scale
-    gate_pre = total[pl.ds(3 * group, group), :] * scale
     lower = floors[...]
     forget = lower + (1.0 - lower) * jax.nn.sigmoid(forget_pre)
     activ = query * jax.nn.sigmoid(query)
@@ -418,24 +448,38 @@
             new = v_row + f_col * (state[s, h] - v_row)
             heads[pl.ds(i, 1), :] = jnp.sum(new * q_col, axis=0, keepdims=True)
 
+    @pl.when(jnp.logical_not(is_special))
+    def _():
+        wait_rows(chunk_in, kv - 1, second, rs_recv.at[1])
+        total[second, :] = add_up(order, second)
+
+    @pl.when(is_special)
+    def _():
+        wait_rows(chunk_in, len(direct) - 1, second, rs_recv.at[1])
+        total[second, :] = add_up(direct, second) + relayed_in[second, :]
+
+    gate_pre = total[second, :] * scale
     head_out = heads[...]
     normed = head_out * lax.rsqrt(jnp.mean(head_out * head_out, axis=1, keepdims=True) + EPS)
     mixed = normed * head_gain[...] * (gate_pre * jax.nn.sigmoid(gate_pre))
-    mix[z] = mixed.astype(BF16)
+    mix_own[...] = mixed.astype(BF16)
     for d in far_first:
-        remote(mix.at[z], mix.at[z], mix_send.at[0], mix_recv.at[0], peer(d), c).start()
+        remote(mix_own, mix.at[z], mix_send.at[0], mix_recv.at[0], peer(d), other).start()
+    remote(mix_own, mix.at[z], mix_send.at[0], mix_recv.at[0], z, other).start()
     tok.wait_send()
     is_relay = (z == relays[0]) | (z == relays[last])
 
     @pl.when(jnp.logical_not(is_relay))
     def _():
         wait_all(sq_in, kv - 1, sq_send.at[0], False)
-        wait_all(chunk_in, kv - 1, rs_send.at[0], False)
+        wait_rows(chunk_in, kv - 1, first, rs_send.at[0], False)
+        wait_rows(chunk_in, kv - 1, second, rs_send.at[1], False)
 
     @pl.when(is_relay)
     def _():
         wait_all(sq_in, kv - 2, sq_send.at[0], False)
-        wait_all(chunk_in, kv - 2, rs_send.at[0], False)
+        wait_rows(chunk_in, kv - 2, first, rs_send.at[0], False)
+        wait_rows(chunk_in, kv - 2, second, rs_send.at[1], False)
         remote(relayed_out, relayed_in, relayed_send.at[0], relayed_recv.at[0], z, other).wait_send()
 
     for h in range(heads_local):
@@ -445,7 +489,7 @@
             value_out[s, pl.ds(h, 1), :] = value[i : i + 1]
     weight_copies[0].wait()
     swaps[0].wait_recv()
-    wait_all(mix, kv - 1, mix_recv.at[0])
+    wait_all(mix, kv, mix_recv.at[0])
     by_head = dot(gather, mix[...].reshape(kv * group, dv)).astype(BF16)
     every = jnp.concatenate([by_head[h * rows : (h + 1) * rows] for h in range(heads_local)], axis=1)
     part_out[...] = packed(dot_t(every, out_w[1]))
@@ -470,7 +514,7 @@
         remote(mid_own, mid.at[half_z * tp + c], mid_send.at[0], mid_recv.at[0], z, half).start()
 
     part.wait_send()
-    wait_all(mix, kv - 1, mix_send.at[0], False)
+    wait_all(mix, kv, mix_send.at[0], False)
     for copy in swaps:
         copy.wait_send()
     gain = mlp_gain[pl.ds(pl.multiple_of(c * half_kv, half_kv), half_kv), :]
@@ -615,6 +659,7 @@
             pltpu.VMEM((kv, seqs, dk), F32),
             pltpu.VMEM((4 * group + 8, dk), F32),
             pltpu.VMEM((4 * group + 8, dk), F32),
+            pltpu.VMEM((group, dv), BF16),
             pltpu.VMEM((kv, group, dv), BF16),
             pltpu.VMEM((rows // 2, 2 * feats), F32),
             pltpu.VMEM((rows // 2, 2 * feats), F32),
@@ -627,7 +672,8 @@
             dma((11,)),
             dma((7,)),
             dma((7,)),
-            *[dma((1,))] * 14,
+            *[dma((2,))] * 2,
+            *[dma((1,))] * 12,
             pltpu.SemaphoreType.REGULAR,
             pltpu.SemaphoreType.REGULAR((kv,)),
         ],

time: 84.9 us -> 86.6 us (1.020)
  Pallas kernels: 82.1 us -> 83.8 us
    pallas_call x1, Pallas kernels: 82.1 us -> 83.8 us  [body(): pl.pallas_call(functools.partial(kernel, kv, tp), name='decode_step', out...]
where the time goes in v6:
time: 86.6 us; the launch traced here: 86.4 us
  Pallas kernels  83.8 us (97%)
  other arithmetic  1.31 us (2%)
    pallas_call x1, Pallas kernels, body(): pl.pallas_call(functools.partial(kernel, kv, tp), name='decode_step', out...  83.8 us

profile of v6, /device:TPU:65, one launch (start us, length us, event | category | flops | bytes accessed | tf_op | source)
XLA Modules:
  0.0 86.4 jit_solution(10171532670538782297)
XLA Ops:
  0.6 0.0 copy-start
  0.6 83.8 %decode_step.1 = (bf16[32,64]{1,0:T(8,128)(2,1)S(1)}, f32[2,8,128]{2,1,0:T(8,128)S(1)}, f32[2,8,128]{2,1,0:T(8,128)S(1)}) custom-call(bf16[32,64]{1,0:T(8,128)(2,1)} %tokens_hbm.1, f32[2,8,128,128]{3,2,1,0:T(8,128)} %past_state.1, f32[1,128]{1,0:T(1,128)} %bitcast.12, bf16[128,1024]{1,0:T(8,128)(2,1)} %w_query.1, bf16[128,1024]{1,0:T(8,128)(2,1)} %w_forget.1, ...), custom_call_target="tpu_custom_call" | custom-call | tf_op jit(solution)/shard_map/decode_step/pallas_call | solution.py:628
  84.5 0.0 copy-done
  84.5 1.3 %multiply_add_fusion = f32[2,8,128,128]{3,2,1,0:T(8,128)} fusion(f32[2,8,128,128]{3,2,1,0:T(8,128)S(1)} %copy-done, f32[2,8,128]{2,1,0:T(8,128)S(1)} %get-tuple-element.7, f32[2,8,128]{2,1,0:T(8,128)S(1)} %get-tuple-element.6), kind=kLoop, calls=%fused_computation | loop fusion | flops 786432 | bytes 2113536 | tf_op jit(solution)/shard_map/add | solution.py:700
  85.8 0.6 copy.17
Async XLA Ops:
  0.6 83.8 %copy-start = (f32[2,8,128,128]{3,2,1,0:T(8,128)S(1)}, f32[2,8,128,128]{3,2,1,0:T(8,128)}, u32[]{:S(2)}) copy-start(f32[2,8,128,128]{3,2,1,0:T(8,128)} %past_state.1) | copy-start | bytes 3145732

commit v7 on v5

--- a/solution.py
+++ b/solution.py
@@ -71,13 +71,11 @@
     heads,
     chunk_out,
     chunk_in,
-    sq_out,
-    sq_in,
     total,
     relay_in,
-    relay_sq_in,
     relayed_out,
     relayed_in,
+    mix_own,
     mix,
     part_out,
     part_in,
@@ -92,8 +90,6 @@
     pair_recv,
     rs_send,
     rs_recv,
-    sq_send,
-    sq_recv,
     mix_send,
     mix_recv,
     mid_send,
@@ -101,7 +97,6 @@
     term_send,
     term_recv,
     relay_recv,
-    relay_sq_recv,
     relayed_send,
     relayed_recv,
     pair_in,
@@ -175,7 +170,7 @@
     half_of = pl.ds(pl.multiple_of(c * half_cols, half_cols), half_cols)
     half_of_other = pl.ds(pl.multiple_of(other * half_cols, half_cols), half_cols)
     weight_copies = [
-        local(w_out.at[:, half_of], out_w.at[0], 7),
+        local(w_out.at[:, half_of_other], out_w.at[0], 7),
         local(w_gate.at[:, half_of], mlp_w.at[0], 8),
         local(w_up.at[:, half_of], mlp_w.at[1], 9),
         local(w_down.at[:, half_of], down_w.at[0], 10),
@@ -248,37 +243,18 @@
     mine = lax.broadcasted_iota(jnp.int32, (rows, tp * feats), 1) // feats == c
     block = jnp.where(mine, own_twice, got_twice)
     squares = jnp.sum(block * block, axis=1, keepdims=True)
-    sq_out[...] = jnp.broadcast_to(squares, (rows, dk)).reshape(kv, seqs, dk)
+    high = squares.astype(BF16).astype(F32)
+    parts = jnp.where(low, high, squares - high).reshape(kv, seqs, dk)
+    chunk_out[:, pl.ds(4 * group, seqs), :] = parts.astype(BF16)
     gain_copy.wait()
     gained = (block * mix_gain[...]).astype(BF16)
-    def sq_copy(to):
-        return remote(sq_out.at[to], sq_in.at[z], sq_send.at[0], sq_recv.at[0], to, c)
-
     def chunk_copy(to):
         return remote(chunk_out.at[to], chunk_in.at[z], rs_send.at[0], rs_recv.at[0], to, c)
-
-    def sq_to_relay(special):
-        return remote(
-            sq_out.at[special], relay_sq_in.at[z - 1], sq_send.at[0], relay_sq_recv.at[0], relays[special], c
-        )
 
     def chunk_to_relay(special):
         return remote(
             chunk_out.at[special], relay_in.at[z - 1], rs_send.at[0], relay_recv.at[0], relays[special], c
         )
-
-    for d in far_first:
-        to = peer(d)
-
-        @pl.when(place(to) < place(z))
-        def _(to=to):
-            sq_copy(to).start()
-
-    for special, relay in relays.items():
-
-        @pl.when((z > relay) & (z <= behind))
-        def _(special=special):
-            sq_to_relay(special).start()
 
     pltpu.make_async_copy(proj_w, proj_w, local_sem.at[0]).wait()
     products = [dot(gained, proj_w[i]).astype(BF16) for i in range(4)]
@@ -310,15 +286,19 @@
             chunk_to_relay(special).start()
 
     swaps = [
-        remote(w_out.at[:, half_of_other], out_w.at[1], pair_send.at[1], pair_recv.at[1], z, other),
+        remote(w_out.at[:, half_of], out_w.at[1], pair_send.at[1], pair_recv.at[1], z, other),
         remote(w_gate.at[:, half_of_other], mlp_w.at[2], pair_send.at[2], pair_recv.at[2], z, other),
         remote(w_up.at[:, half_of_other], mlp_w.at[3], pair_send.at[3], pair_recv.at[3], z, other),
         remote(w_down.at[:, half_of_other], down_w.at[1], pair_send.at[4], pair_recv.at[4], z, other),
     ]
-    for s in swaps:
-        s.start()
-
-    sq_in[z] = sq_out[z]
+    is_special = (z == 0) | (z == last)
+
+    @pl.when(jnp.logical_not(is_special))
+    def _():
+        for s in swaps:
+            s.start()
+
+
     chunk_in[z] = chunk_out[z]
     for copy in small_copies:
         copy.wait()
@@ -331,11 +311,9 @@
         @pl.when(place(z) < place(w))
         def _(w=w):
             pl.semaphore_wait(ready.at[w], 1)
-            sq_copy(w).start()
             chunk_copy(w).start()
             for special, relay in relays.items():
                 if relay == w:
-                    sq_to_relay(special).start()
                     chunk_to_relay(special).start()
 
     for special, relay in relays.items():
@@ -343,17 +321,12 @@
 
         @pl.when(z == relay)
         def _(special=special, forward=forward):
-            wait_all(relay_sq_in, behind - 1, relay_sq_recv.at[0])
             wait_all(relay_in, behind - 1, relay_recv.at[0])
-            relay_sq_in[z - 1] = sq_out[special]
             relay_in[z - 1] = chunk_out[special]
             sums = relay_in[0].astype(F32)
-            squares = relay_sq_in[0]
             for i in range(1, behind):
                 sums = sums + relay_in[i].astype(F32)
-                squares = squares + relay_sq_in[i]
-            relayed_out[pl.ds(0, 4 * group), :] = sums
-            relayed_out[pl.ds(4 * group, seqs), :] = squares
+            relayed_out[...] = sums
             pl.semaphore_wait(ready.at[special], 1)
             forward.start()
 
@@ -363,37 +336,31 @@
                 @pl.when(z == w)
                 def _(special=special):
                     pl.semaphore_wait(ready.at[special], 1)
-                    sq_copy(special).start()
                     chunk_copy(special).start()
 
     def add_up(slots):
         sums = chunk_in[slots[0]].astype(F32)
-        squares = sq_in[slots[0]]
         for w in slots[1:]:
             sums = sums + chunk_in[w].astype(F32)
-            squares = squares + sq_in[w]
-        return sums, squares
-
-    is_special = (z == 0) | (z == last)
+        return sums
+
+    direct = [*near_last, 0, last]
 
     @pl.when(jnp.logical_not(is_special))
     def _():
-        wait_all(sq_in, kv - 1, sq_recv.at[0])
         wait_all(chunk_in, kv - 1, rs_recv.at[0])
-        sums, squares = add_up(order)
-        total[pl.ds(0, 4 * group), :] = sums
-        total[pl.ds(4 * group, seqs), :] = squares
+        total[...] = add_up(order)
 
     @pl.when(is_special)
     def _():
-        wait_all(sq_in, len(near_last) + 1, sq_recv.at[0])
-        wait_all(chunk_in, len(near_last) + 1, rs_recv.at[0])
-        sums, squares = add_up([*near_last, 0, last])
+        wait_all(chunk_in, len(direct) - 1, rs_recv.at[0])
         remote(relayed_out, relayed_in, relayed_send.at[0], relayed_recv.at[0], z, other).wait_recv()
-        total[pl.ds(0, 4 * group), :] = sums + relayed_in[pl.ds(0, 4 * group), :]
-        total[pl.ds(4 * group, seqs), :] = squares + relayed_in[pl.ds(4 * group, seqs), :]
+        total[...] = add_up(direct) + relayed_in[...]
+        for s in swaps:
+            s.start()
 
     total_sq = total[pl.ds(4 * group, seqs), :]
+    total_sq = total_sq + halves_swapped(total_sq)
     scale_s = lax.rsqrt(total_sq / width + EPS)
     row_of = lax.broadcasted_iota(jnp.int32, (group, dk), 0)
     scale = jnp.broadcast_to(scale_s[0:1], (group, dk))
@@ -421,20 +388,19 @@
     head_out = heads[...]
     normed = head_out * lax.rsqrt(jnp.mean(head_out * head_out, axis=1, keepdims=True) + EPS)
     mixed = normed * head_gain[...] * (gate_pre * jax.nn.sigmoid(gate_pre))
-    mix[z] = mixed.astype(BF16)
+    mix_own[...] = mixed.astype(BF16)
     for d in far_first:
-        remote(mix.at[z], mix.at[z], mix_send.at[0], mix_recv.at[0], peer(d), c).start()
+        remote(mix_own, mix.at[z], mix_send.at[0], mix_recv.at[0], peer(d), other).start()
+    remote(mix_own, mix.at[z], mix_send.at[0], mix_recv.at[0], z, other).start()
     tok.wait_send()
     is_relay = (z == relays[0]) | (z == relays[last])
 
     @pl.when(jnp.logical_not(is_relay))
     def _():
-        wait_all(sq_in, kv - 1, sq_send.at[0], False)
         wait_all(chunk_in, kv - 1, rs_send.at[0], False)
 
     @pl.when(is_relay)
     def _():
-        wait_all(sq_in, kv - 2, sq_send.at[0], False)
         wait_all(chunk_in, kv - 2, rs_send.at[0], False)
         remote(relayed_out, relayed_in, relayed_send.at[0], relayed_recv.at[0], z, other).wait_send()
 
@@ -445,7 +411,7 @@
             value_out[s, pl.ds(h, 1), :] = value[i : i + 1]
     weight_copies[0].wait()
     swaps[0].wait_recv()
-    wait_all(mix, kv - 1, mix_recv.at[0])
+    wait_all(mix, kv, mix_recv.at[0])
     by_head = dot(gather, mix[...].reshape(kv * group, dv)).astype(BF16)
     every = jnp.concatenate([by_head[h * rows : (h + 1) * rows] for h in range(heads_local)], axis=1)
     part_out[...] = packed(dot_t(every, out_w[1]))
@@ -470,7 +436,7 @@
         remote(mid_own, mid.at[half_z * tp + c], mid_send.at[0], mid_recv.at[0], z, half).start()
 
     part.wait_send()
-    wait_all(mix, kv - 1, mix_send.at[0], False)
+    wait_all(mix, kv, mix_send.at[0], False)
     for copy in swaps:
         copy.wait_send()
     gain = mlp_gain[pl.ds(pl.multiple_of(c * half_kv, half_kv), half_kv), :]
@@ -606,15 +572,13 @@
             pltpu.VMEM((2, units, half_cols), BF16),
             pltpu.VMEM((group, dk), F32),
             pltpu.VMEM((group, dv), F32),
-            pltpu.VMEM((kv, 4 * group, dk), BF16),
-            pltpu.VMEM((kv, 4 * group, dk), BF16),
-            pltpu.VMEM((kv, seqs, dk), F32),
-            pltpu.VMEM((kv, seqs, dk), F32),
-            pltpu.VMEM((4 * group + 8, dk), F32),
-            pltpu.VMEM((kv, 4 * group, dk), BF16),
-            pltpu.VMEM((kv, seqs, dk), F32),
-            pltpu.VMEM((4 * group + 8, dk), F32),
-            pltpu.VMEM((4 * group + 8, dk), F32),
+            pltpu.VMEM((kv, 4 * group + seqs, dk), BF16),
+            pltpu.VMEM((kv, 4 * group + seqs, dk), BF16),
+            pltpu.VMEM((4 * group + seqs, dk), F32),
+            pltpu.VMEM((kv, 4 * group + seqs, dk), BF16),
+            pltpu.VMEM((4 * group + seqs, dk), F32),
+            pltpu.VMEM((4 * group + seqs, dk), F32),
+            pltpu.VMEM((group, dv), BF16),
             pltpu.VMEM((kv, group, dv), BF16),
             pltpu.VMEM((rows // 2, 2 * feats), F32),
             pltpu.VMEM((rows // 2, 2 * feats), F32),
@@ -627,7 +591,7 @@
             dma((11,)),
             dma((7,)),
             dma((7,)),
-            *[dma((1,))] * 14,
+            *[dma((1,))] * 11,
             pltpu.SemaphoreType.REGULAR,
             pltpu.SemaphoreType.REGULAR((kv,)),
         ],

time: 84.9 us -> 85.1 us (level)
  no operation moved by 1% of the time
where the time goes in v7:
time: 85.1 us; the launch traced here: 84.9 us
  Pallas kernels  82.3 us (97%)
  other arithmetic  1.31 us (2%)
    pallas_call x1, Pallas kernels, body(): pl.pallas_call(functools.partial(kernel, kv, tp), name='decode_step', out...  82.3 us

profile of v7, /device:TPU:65, one launch (start us, length us, event | category | flops | bytes accessed | tf_op | source)
XLA Modules:
  0.0 84.9 jit_solution(12108780421194659566)
XLA Ops:
  0.6 0.0 copy-start
  0.6 82.3 %decode_step.1 = (bf16[32,64]{1,0:T(8,128)(2,1)S(1)}, f32[2,8,128]{2,1,0:T(8,128)S(1)}, f32[2,8,128]{2,1,0:T(8,128)S(1)}) custom-call(bf16[32,64]{1,0:T(8,128)(2,1)} %tokens_hbm.1, f32[2,8,128,128]{3,2,1,0:T(8,128)} %past_state.1, f32[1,128]{1,0:T(1,128)} %bitcast.12, bf16[128,1024]{1,0:T(8,128)(2,1)} %w_query.1, bf16[128,1024]{1,0:T(8,128)(2,1)} %w_forget.1, ...), custom_call_target="tpu_custom_call" | custom-call | tf_op jit(solution)/shard_map/decode_step/pallas_call | solution.py:550
  83.0 0.0 copy-done
  83.0 1.3 %multiply_add_fusion = f32[2,8,128,128]{3,2,1,0:T(8,128)} fusion(f32[2,8,128,128]{3,2,1,0:T(8,128)S(1)} %copy-done, f32[2,8,128]{2,1,0:T(8,128)S(1)} %get-tuple-element.7, f32[2,8,128]{2,1,0:T(8,128)S(1)} %get-tuple-element.6), kind=kLoop, calls=%fused_computation | loop fusion | flops 786432 | bytes 2113536 | tf_op jit(solution)/shard_map/add | solution.py:618
  84.3 0.6 copy.17
Async XLA Ops:
  0.6 82.3 %copy-start = (f32[2,8,128,128]{3,2,1,0:T(8,128)S(1)}, f32[2,8,128,128]{3,2,1,0:T(8,128)}, u32[]{:S(2)}) copy-start(f32[2,8,128,128]{3,2,1,0:T(8,128)} %past_state.1) | copy-start | bytes 3145732

commit v8 on v5

--- a/solution.py
+++ b/solution.py
@@ -53,8 +53,7 @@
     w_up,
     w_down,
     result,
-    forget_out,
-    value_out,
+    new_state,
     tokens,
     mix_gain,
     floor_logits,
@@ -78,6 +77,7 @@
     relay_sq_in,
     relayed_out,
     relayed_in,
+    mix_own,
     mix,
     part_out,
     part_in,
@@ -175,7 +175,7 @@
     half_of = pl.ds(pl.multiple_of(c * half_cols, half_cols), half_cols)
     half_of_other = pl.ds(pl.multiple_of(other * half_cols, half_cols), half_cols)
     weight_copies = [
-        local(w_out.at[:, half_of], out_w.at[0], 7),
+        local(w_out.at[:, half_of_other], out_w.at[0], 7),
         local(w_gate.at[:, half_of], mlp_w.at[0], 8),
         local(w_up.at[:, half_of], mlp_w.at[1], 9),
         local(w_down.at[:, half_of], down_w.at[0], 10),
@@ -195,32 +195,37 @@
             def _(w=w):
                 signal(barrier, w, 1)
 
-    @pl.when(c == 1)
-    def _():
-        @pl.when(place(z) > 0)
+    def count_and_tell():
+        @pl.when(c == 1)
         def _():
-            pl.semaphore_wait(barrier, place(z))
-
-        signal(pair_in, z, 0)
-
-    @pl.when(c == 0)
-    def _():
-        pl.semaphore_wait(pair_in, 1)
-
-    for special, told in listeners.items():
-
-        @pl.when(z == special)
-        def _(special=special, told=told):
-            for w in told:
-                if order.index(w) < order.index(special):
-                    signal(ready.at[special], w, c)
-
-    for d in far_first:
-        to = peer(d)
-
-        @pl.when((place(to) < place(z)) & (place(z) < kv - 2))
-        def _(to=to):
-            signal(ready.at[z], to, c)
+            @pl.when(place(z) > 0)
+            def _():
+                pl.semaphore_wait(barrier, place(z))
+
+            signal(pair_in, z, 0)
+
+        @pl.when(c == 0)
+        def _():
+            pl.semaphore_wait(pair_in, 1)
+
+        for special, told in listeners.items():
+
+            @pl.when(z == special)
+            def _(special=special, told=told):
+                for w in told:
+                    if order.index(w) < order.index(special):
+                        signal(ready.at[special], w, c)
+
+        for d in far_first:
+            to = peer(d)
+
+            @pl.when((place(to) < place(z)) & (place(z) < kv - 2))
+            def _(to=to):
+                signal(ready.at[z], to, c)
+
+    @pl.when(z != last)
+    def _():
+        count_and_tell()
 
     tokens_copy.wait()
     own = tokens[...].astype(F32)
@@ -240,6 +245,11 @@
     low = lane < feats
     own_twice = jnp.concatenate([own, own], axis=1)
     tok.wait_recv()
+
+    @pl.when(z == last)
+    def _():
+        count_and_tell()
+
     got = tok_other[...].astype(F32)
     got_swapped = halves_swapped(got)
     got_twice = jnp.concatenate(
@@ -310,13 +320,18 @@
             chunk_to_relay(special).start()
 
     swaps = [
-        remote(w_out.at[:, half_of_other], out_w.at[1], pair_send.at[1], pair_recv.at[1], z, other),
+        remote(w_out.at[:, half_of], out_w.at[1], pair_send.at[1], pair_recv.at[1], z, other),
         remote(w_gate.at[:, half_of_other], mlp_w.at[2], pair_send.at[2], pair_recv.at[2], z, other),
         remote(w_up.at[:, half_of_other], mlp_w.at[3], pair_send.at[3], pair_recv.at[3], z, other),
         remote(w_down.at[:, half_of_other], down_w.at[1], pair_send.at[4], pair_recv.at[4], z, other),
     ]
-    for s in swaps:
-        s.start()
+    is_special = (z == 0) | (z == last)
+
+    @pl.when(jnp.logical_not(is_special))
+    def _():
+        for s in swaps:
+            s.start()
+
 
     sq_in[z] = sq_out[z]
     chunk_in[z] = chunk_out[z]
@@ -392,6 +407,8 @@
         remote(relayed_out, relayed_in, relayed_send.at[0], relayed_recv.at[0], z, other).wait_recv()
         total[pl.ds(0, 4 * group), :] = sums + relayed_in[pl.ds(0, 4 * group), :]
         total[pl.ds(4 * group, seqs), :] = squares + relayed_in[pl.ds(4 * group, seqs), :]
+        for s in swaps:
+            s.start()
 
     total_sq = total[pl.ds(4 * group, seqs), :]
     scale_s = lax.rsqrt(total_sq / width + EPS)
@@ -416,14 +433,16 @@
             f_col = columns[:, i : i + 1]
             q_col = columns[:, group + i : group + i + 1]
             new = v_row + f_col * (state[s, h] - v_row)
+            new_state[s, h] = new
             heads[pl.ds(i, 1), :] = jnp.sum(new * q_col, axis=0, keepdims=True)
 
     head_out = heads[...]
     normed = head_out * lax.rsqrt(jnp.mean(head_out * head_out, axis=1, keepdims=True) + EPS)
     mixed = normed * head_gain[...] * (gate_pre * jax.nn.sigmoid(gate_pre))
-    mix[z] = mixed.astype(BF16)
+    mix_own[...] = mixed.astype(BF16)
     for d in far_first:
-        remote(mix.at[z], mix.at[z], mix_send.at[0], mix_recv.at[0], peer(d), c).start()
+        remote(mix_own, mix.at[z], mix_send.at[0], mix_recv.at[0], peer(d), other).start()
+    remote(mix_own, mix.at[z], mix_send.at[0], mix_recv.at[0], z, other).start()
     tok.wait_send()
     is_relay = (z == relays[0]) | (z == relays[last])
 
@@ -438,14 +457,9 @@
         wait_all(chunk_in, kv - 2, rs_send.at[0], False)
         remote(relayed_out, relayed_in, relayed_send.at[0], relayed_recv.at[0], z, other).wait_send()
 
-    for h in range(heads_local):
-        for s in range(seqs):
-            i = h * seqs + s
-            forget_out[s, pl.ds(h, 1), :] = forget[i : i + 1]
-            value_out[s, pl.ds(h, 1), :] = value[i : i + 1]
     weight_copies[0].wait()
     swaps[0].wait_recv()
-    wait_all(mix, kv - 1, mix_recv.at[0])
+    wait_all(mix, kv, mix_recv.at[0])
     by_head = dot(gather, mix[...].reshape(kv * group, dv)).astype(BF16)
     every = jnp.concatenate([by_head[h * rows : (h + 1) * rows] for h in range(heads_local)], axis=1)
     part_out[...] = packed(dot_t(every, out_w[1]))
@@ -470,7 +484,7 @@
         remote(mid_own, mid.at[half_z * tp + c], mid_send.at[0], mid_recv.at[0], z, half).start()
 
     part.wait_send()
-    wait_all(mix, kv - 1, mix_send.at[0], False)
+    wait_all(mix, kv, mix_send.at[0], False)
     for copy in swaps:
         copy.wait_send()
     gain = mlp_gain[pl.ds(pl.multiple_of(c * half_kv, half_kv), half_kv), :]
@@ -504,15 +518,10 @@
     sq_bottom = jnp.sum(jnp.where(low, 0.0, squares), axis=1, keepdims=True)
     sq_mid = jnp.concatenate([sq_top, sq_bottom], axis=0)
     wide_out[4, :, :] = jnp.broadcast_to(sq_mid, wide_out.shape[1:])
-    wides = [
-        remote(wide_out.at[i], wide_in.at[i], pair_send.at[6], pair_recv.at[6], z, other) for i in range(5)
-    ]
-    wides[4].start()
-    sums = []
+    sums = [dot_t(features, mlp_w[i]) for i in range(4)]
     for i in range(4):
-        sums.append(dot_t(features, mlp_w[i]))
         wide_out[i, :, pl.ds(0, units)] = sums[i]
-        wides[i].start()
+    remote(wide_out, wide_in, pair_send.at[6], pair_recv.at[6], z, other).start()
     remote(wide_out, wide_in, pair_send.at[6], pair_recv.at[6], z, other).wait_recv()
     mlp_scale = lax.rsqrt((sq_mid + wide_in[4, :, 0:1]) / width + EPS)
     terms = None
@@ -552,6 +561,17 @@
     result[pl.ds(half_rows, half_rows), :] = summed[:, feats:].astype(BF16)
 
     wait_others(terms_in, term_send.at[0], False)
+
+
+def write_out(result, new_state, result_out, new_state_out, sem):
+    copies = [
+        pltpu.make_async_copy(new_state, new_state_out, sem.at[0]),
+        pltpu.make_async_copy(result, result_out, sem.at[1]),
+    ]
+    for copy in copies:
+        copy.start()
+    for copy in copies:
+        copy.wait()
 
 
 def body(
@@ -581,16 +601,15 @@
     wide = -(-units // 128) * 128
     in_vmem = pl.BlockSpec(memory_space=pltpu.VMEM)
     dma = pltpu.SemaphoreType.DMA
-    result, forget, value = pl.pallas_call(
+    outputs = pl.pallas_call(
         functools.partial(kernel, kv, tp),
         name="decode_step",
         out_shape=(
             jax.ShapeDtypeStruct((rows, feats), BF16),
-            jax.ShapeDtypeStruct((seqs, heads_local, dk), F32),
-            jax.ShapeDtypeStruct((seqs, heads_local, dv), F32),
+            jax.ShapeDtypeStruct(past_state.shape, F32),
         ),
         in_specs=[pl.BlockSpec(memory_space=pltpu.HBM)] * 14,
-        out_specs=(in_vmem, in_vmem, in_vmem),
+        out_specs=(in_vmem, in_vmem),
         scratch_shapes=[
             pltpu.VMEM((rows, feats), BF16),
             pltpu.VMEM((1, tp * feats), F32),
@@ -615,6 +634,7 @@
             pltpu.VMEM((kv, seqs, dk), F32),
             pltpu.VMEM((4 * group + 8, dk), F32),
             pltpu.VMEM((4 * group + 8, dk), F32),
+            pltpu.VMEM((group, dv), BF16),
             pltpu.VMEM((kv, group, dv), BF16),
             pltpu.VMEM((rows // 2, 2 * feats), F32),
             pltpu.VMEM((rows // 2, 2 * feats), F32),
@@ -650,8 +670,15 @@
         w_up.T,
         w_down,
     ))
-    value = value[:, :, None, :]
-    return result, value + forget[..., None] * (past_state - value)
+    return pl.pallas_call(
+        write_out,
+        name="write_out",
+        out_shape=tuple(jax.ShapeDtypeStruct(a.shape, a.dtype) for a in outputs),
+        in_specs=[in_vmem] * len(outputs),
+        out_specs=(pl.BlockSpec(memory_space=pltpu.HBM),) * len(outputs),
+        scratch_shapes=[dma((len(outputs),))],
+        compiler_params=pltpu.CompilerParams(vmem_limit_bytes=16 * 1024 * 1024),
+    )(*outputs)
 
 
 def solution(mesh):

time: 84.9 us -> 82.9 us (0.976)
  other arithmetic: 1.31 us -> 0 us
    add x1 -> x0, other arithmetic: 1.31 us -> none  [body(): return (result, value + forget[..., None] * (past_state - value))]
    pallas_call x1, Pallas kernels: 82.1 us -> 81.1 us  [body(): pl.pallas_call(functools.partial(kernel, kv, tp), name='decode_step', out...]
    pallas_call x0 -> x1, Pallas kernels: none -> 0.99 us  [body(): pl.pallas_call(write_out, name='write_out', out_shape=tuple((jax.ShapeDty...]
where the time goes in v8:
time: 82.9 us; the launch traced here: 82.7 us
  Pallas kernels  82.1 us (99%)
    pallas_call x1, Pallas kernels, body(): pl.pallas_call(functools.partial(kernel, kv, tp), name='decode_step', out...  81.1 us

profile of v8, /device:TPU:65, one launch (start us, length us, event | category | flops | bytes accessed | tf_op | source)
XLA Modules:
  0.0 82.7 jit_solution(3960861818627658840)
XLA Ops:
  0.6 81.1 %decode_step.1 = (bf16[32,64]{1,0:T(8,128)(2,1)S(1)}, f32[2,8,128,128]{3,2,1,0:T(8,128)S(1)}) custom-call(bf16[32,64]{1,0:T(8,128)(2,1)} %tokens_hbm.1, f32[2,8,128,128]{3,2,1,0:T(8,128)} %past_state.1, f32[1,128]{1,0:T(1,128)} %bitcast.12, bf16[128,1024]{1,0:T(8,128)(2,1)} %w_query.1, bf16[128,1024]{1,0:T(8,128)(2,1)} %w_forget.1, ...), custom_call_target="tpu_custom_call" | custom-call | tf_op jit(solution)/shard_map/decode_step/pallas_call | solution.py:604
  81.7 1.0 %write_out.1 = (bf16[32,64]{1,0:T(8,128)(2,1)}, f32[2,8,128,128]{3,2,1,0:T(8,128)}) custom-call(bf16[32,64]{1,0:T(8,128)(2,1)S(1)} %get-tuple-element.4.result, f32[2,8,128,128]{3,2,1,0:T(8,128)S(1)} %get-tuple-element.5.new_state), custom_call_target="tpu_custom_call" | custom-call | tf_op jit(solution)/shard_map/write_out/pallas_call | solution.py:673

commit v9 on v8

--- a/solution.py
+++ b/solution.py
@@ -195,7 +195,7 @@
             def _(w=w):
                 signal(barrier, w, 1)
 
-    def count_and_tell():
+    def count():
         @pl.when(c == 1)
         def _():
             @pl.when(place(z) > 0)
@@ -208,24 +208,23 @@
         def _():
             pl.semaphore_wait(pair_in, 1)
 
-        for special, told in listeners.items():
-
-            @pl.when(z == special)
-            def _(special=special, told=told):
-                for w in told:
-                    if order.index(w) < order.index(special):
-                        signal(ready.at[special], w, c)
-
+    def count_and_tell_listeners(special):
+        @pl.when(z == special)
+        def _():
+            count()
+            for w in listeners[special]:
+                if order.index(w) < order.index(special):
+                    signal(ready.at[special], w, c)
+
+    @pl.when((z != 0) & (z != last))
+    def _():
+        count()
         for d in far_first:
             to = peer(d)
 
-            @pl.when((place(to) < place(z)) & (place(z) < kv - 2))
+            @pl.when(place(to) < place(z))
             def _(to=to):
                 signal(ready.at[z], to, c)
-
-    @pl.when(z != last)
-    def _():
-        count_and_tell()
 
     tokens_copy.wait()
     own = tokens[...].astype(F32)
@@ -246,10 +245,7 @@
     own_twice = jnp.concatenate([own, own], axis=1)
     tok.wait_recv()
 
-    @pl.when(z == last)
-    def _():
-        count_and_tell()
-
+    count_and_tell_listeners(last)
     got = tok_other[...].astype(F32)
     got_swapped = halves_swapped(got)
     got_twice = jnp.concatenate(
@@ -276,19 +272,6 @@
         return remote(
             chunk_out.at[special], relay_in.at[z - 1], rs_send.at[0], relay_recv.at[0], relays[special], c
         )
-
-    for d in far_first:
-        to = peer(d)
-
-        @pl.when(place(to) < place(z))
-        def _(to=to):
-            sq_copy(to).start()
-
-    for special, relay in relays.items():
-
-        @pl.when((z > relay) & (z <= behind))
-        def _(special=special):
-            sq_to_relay(special).start()
 
     pltpu.make_async_copy(proj_w, proj_w, local_sem.at[0]).wait()
     products = [dot(gained, proj_w[i]).astype(BF16) for i in range(4)]
@@ -306,17 +289,21 @@
                 kv, group, dk
             )
 
+    count_and_tell_listeners(0)
+
     for d in far_first:
         to = peer(d)
 
         @pl.when(place(to) < place(z))
         def _(to=to):
+            sq_copy(to).start()
             chunk_copy(to).start()
 
     for special, relay in relays.items():
 
         @pl.when((z > relay) & (z <= behind))
         def _(special=special):
+            sq_to_relay(special).start()
             chunk_to_relay(special).start()
 
     swaps = [
@@ -535,23 +522,28 @@
     for i in range(half_kv):
         at = slice(i * tp * feats, (i + 1) * tp * feats)
         top, bottom = terms[:half_rows, at], terms[half_rows:, at]
-        to = c * half_kv + i
         for to_c, message in (
             (0, jnp.where(low, top, halves_swapped(bottom))),
             (1, jnp.where(low, halves_swapped(top), bottom)),
         ):
-            n = 2 * i + to_c
-            terms_out[n] = message.astype(BF16)
-            copy = remote(terms_out.at[n], terms_in.at[z], term_send.at[0], term_recv.at[0], to, to_c)
-            to_self = jnp.logical_and(to == z, to_c == c)
-
-            @pl.when(jnp.logical_not(to_self))
-            def _(copy=copy):
-                copy.start()
-
-            @pl.when(to_self)
-            def _(n=n):
-                terms_in[z] = terms_out[n]
+            terms_out[tp * i + to_c] = message.astype(BF16)
+
+    def term_copy(to, to_c):
+        n = tp * (to - c * half_kv) + to_c
+        return remote(terms_out.at[n], terms_in.at[z], term_send.at[0], term_recv.at[0], to, to_c)
+
+    for d in far_first:
+        to = peer(d)
+
+        @pl.when(to // half_kv == c)
+        def _(to=to):
+            for to_c in range(tp):
+                term_copy(to, to_c).start()
+
+    @pl.when(kept_here)
+    def _():
+        term_copy(z, other).start()
+        terms_in[z] = terms_out[tp * (z - c * half_kv) + c]
 
     remote(wide_out, wide_in, pair_send.at[6], pair_recv.at[6], z, other).wait_send()
     wait_others(mid, mid_send.at[0], False)

time: 82.9 us -> 84.9 us (1.024)
  Pallas kernels: 82.1 us -> 84.1 us
    pallas_call x1, Pallas kernels: 81.1 us -> 83.1 us  [body(): pl.pallas_call(functools.partial(kernel, kv, tp), name='decode_step', out...]
where the time goes in v9:
time: 84.9 us; the launch traced here: 84.8 us
  Pallas kernels  84.1 us (99%)
    pallas_call x1, Pallas kernels, body(): pl.pallas_call(functools.partial(kernel, kv, tp), name='decode_step', out...  83.1 us

profile of v9, /device:TPU:65, one launch (start us, length us, event | category | flops | bytes accessed | tf_op | source)
XLA Modules:
  0.0 84.8 jit_solution(7946698522891514155)
XLA Ops:
  0.6 83.1 %decode_step.1 = (bf16[32,64]{1,0:T(8,128)(2,1)S(1)}, f32[2,8,128,128]{3,2,1,0:T(8,128)S(1)}) custom-call(bf16[32,64]{1,0:T(8,128)(2,1)} %tokens_hbm.1, f32[2,8,128,128]{3,2,1,0:T(8,128)} %past_state.1, f32[1,128]{1,0:T(1,128)} %bitcast.12, bf16[128,1024]{1,0:T(8,128)(2,1)} %w_query.1, bf16[128,1024]{1,0:T(8,128)(2,1)} %w_forget.1, ...), custom_call_target="tpu_custom_call" | custom-call | tf_op jit(solution)/shard_map/decode_step/pallas_call | solution.py:596
  83.8 1.0 %write_out.1 = (bf16[32,64]{1,0:T(8,128)(2,1)}, f32[2,8,128,128]{3,2,1,0:T(8,128)}) custom-call(bf16[32,64]{1,0:T(8,128)(2,1)S(1)} %get-tuple-element.4.result, f32[2,8,128,128]{3,2,1,0:T(8,128)S(1)} %get-tuple-element.5.new_state), custom_call_target="tpu_custom_call" | custom-call | tf_op jit(solution)/shard_map/write_out/pallas_call | solution.py:665

commit v10 on v8

--- a/solution.py
+++ b/solution.py
@@ -73,6 +73,7 @@
     sq_out,
     sq_in,
     total,
+    joint_in,
     relay_in,
     relay_sq_in,
     relayed_out,
@@ -100,6 +101,7 @@
     mid_recv,
     term_send,
     term_recv,
+    joint_recv,
     relay_recv,
     relay_sq_recv,
     relayed_send,
@@ -172,6 +174,7 @@
         local(head_gain_hbm, head_gain, 5),
         local(mlp_gain_hbm, mlp_gain, 6),
     ]
+    is_special = (z == 0) | (z == last)
     half_of = pl.ds(pl.multiple_of(c * half_cols, half_cols), half_cols)
     half_of_other = pl.ds(pl.multiple_of(other * half_cols, half_cols), half_cols)
     weight_copies = [
@@ -309,7 +312,7 @@
     for d in far_first:
         to = peer(d)
 
-        @pl.when(place(to) < place(z))
+        @pl.when((place(to) < place(z)) & jnp.logical_not(is_special))
         def _(to=to):
             chunk_copy(to).start()
 
@@ -325,8 +328,6 @@
         remote(w_up.at[:, half_of_other], mlp_w.at[3], pair_send.at[3], pair_recv.at[3], z, other),
         remote(w_down.at[:, half_of_other], down_w.at[1], pair_send.at[4], pair_recv.at[4], z, other),
     ]
-    is_special = (z == 0) | (z == last)
-
     @pl.when(jnp.logical_not(is_special))
     def _():
         for s in swaps:
@@ -381,11 +382,29 @@
                     sq_copy(special).start()
                     chunk_copy(special).start()
 
-    def add_up(slots):
+    middle_z = kv // 2
+    sides = {0: list(range(middle_z, 0, -1)), last: list(range(middle_z + 1, last))}
+    for special, partner in ((last, 0), (0, last)):
+
+        @pl.when(z == special)
+        def _(special=special, partner=partner):
+            for w in sides[partner]:
+                remote(
+                    chunk_out.at[w], joint_in.at[w], rs_send.at[0], joint_recv.at[w], partner, c
+                ).start()
+            if special == last:
+                chunk_copy(partner).start()
+            for w in sides[special]:
+                remote(joint_in.at[w], joint_in.at[w], joint_recv.at[w], joint_recv.at[w], z, other).wait_recv()
+                chunk_out[w] = (chunk_out[w].astype(F32) + joint_in[w].astype(F32)).astype(BF16)
+                remote(chunk_out.at[w], chunk_in.at[0], rs_send.at[0], rs_recv.at[0], w, c).start()
+
+    def add_up(slots, joint):
         sums = chunk_in[slots[0]].astype(F32)
         squares = sq_in[slots[0]]
         for w in slots[1:]:
-            sums = sums + chunk_in[w].astype(F32)
+            if not (joint and w == last):
+                sums = sums + chunk_in[w].astype(F32)
             squares = squares + sq_in[w]
         return sums, squares
 
@@ -394,8 +413,8 @@
     @pl.when(jnp.logical_not(is_special))
     def _():
         wait_all(sq_in, kv - 1, sq_recv.at[0])
-        wait_all(chunk_in, kv - 1, rs_recv.at[0])
-        sums, squares = add_up(order)
+        wait_all(chunk_in, kv - 2, rs_recv.at[0])
+        sums, squares = add_up(order, True)
         total[pl.ds(0, 4 * group), :] = sums
         total[pl.ds(4 * group, seqs), :] = squares
 
@@ -403,7 +422,7 @@
     def _():
         wait_all(sq_in, len(near_last) + 1, sq_recv.at[0])
         wait_all(chunk_in, len(near_last) + 1, rs_recv.at[0])
-        sums, squares = add_up([*near_last, 0, last])
+        sums, squares = add_up([*near_last, 0, last], False)
         remote(relayed_out, relayed_in, relayed_send.at[0], relayed_recv.at[0], z, other).wait_recv()
         total[pl.ds(0, 4 * group), :] = sums + relayed_in[pl.ds(0, 4 * group), :]
         total[pl.ds(4 * group, seqs), :] = squares + relayed_in[pl.ds(4 * group, seqs), :]
@@ -631,6 +650,7 @@
             pltpu.VMEM((kv, seqs, dk), F32),
             pltpu.VMEM((4 * group + 8, dk), F32),
             pltpu.VMEM((kv, 4 * group, dk), BF16),
+            pltpu.VMEM((kv, 4 * group, dk), BF16),
             pltpu.VMEM((kv, seqs, dk), F32),
             pltpu.VMEM((4 * group + 8, dk), F32),
             pltpu.VMEM((4 * group + 8, dk), F32),
@@ -647,7 +667,9 @@
             dma((11,)),
             dma((7,)),
             dma((7,)),
-            *[dma((1,))] * 14,
+            *[dma((1,))] * 10,
+            dma((kv,)),
+            *[dma((1,))] * 4,
             pltpu.SemaphoreType.REGULAR,
             pltpu.SemaphoreType.REGULAR((kv,)),
         ],

time: 82.9 us -> 82.6 us (level)
  no operation moved by 1% of the time
where the time goes in v10:
time: 82.6 us; the launch traced here: 82.4 us
  Pallas kernels  81.8 us (99%)
    pallas_call x1, Pallas kernels, body(): pl.pallas_call(functools.partial(kernel, kv, tp), name='decode_step', out...  80.8 us

profile of v10, /device:TPU:65, one launch (start us, length us, event | category | flops | bytes accessed | tf_op | source)
XLA Modules:
  0.0 82.4 jit_solution(3026725981300075777)
XLA Ops:
  0.6 80.8 %decode_step.1 = (bf16[32,64]{1,0:T(8,128)(2,1)S(1)}, f32[2,8,128,128]{3,2,1,0:T(8,128)S(1)}) custom-call(bf16[32,64]{1,0:T(8,128)(2,1)} %tokens_hbm.1, f32[2,8,128,128]{3,2,1,0:T(8,128)} %past_state.1, f32[1,128]{1,0:T(1,128)} %bitcast.12, bf16[128,1024]{1,0:T(8,128)(2,1)} %w_query.1, bf16[128,1024]{1,0:T(8,128)(2,1)} %w_forget.1, ...), custom_call_target="tpu_custom_call" | custom-call | tf_op jit(solution)/shard_map/decode_step/pallas_call | solution.py:623
  81.4 1.0 %write_out.1 = (bf16[32,64]{1,0:T(8,128)(2,1)}, f32[2,8,128,128]{3,2,1,0:T(8,128)}) custom-call(bf16[32,64]{1,0:T(8,128)(2,1)S(1)} %get-tuple-element.4.result, f32[2,8,128,128]{3,2,1,0:T(8,128)S(1)} %get-tuple-element.5.new_state), custom_call_target="tpu_custom_call" | custom-call | tf_op jit(solution)/shard_map/write_out/pallas_call | solution.py:695

commit v11 on v10

--- a/solution.py
+++ b/solution.py
@@ -145,6 +145,8 @@
     order = [*range(1, kv - 1), 0, kv - 1]
     last = kv - 1
     near_last = [w for w in range(kv - tp - 2, kv - 1)]
+    middle_z = kv // 2
+    far_side = list(range(middle_z - 2, middle_z + 2))
     relays = {0: kv // 4, last: near_last[0] - 1}
     behind = near_last[0] - 1
     listeners = {0: [relays[0], *near_last], last: [relays[last], *near_last, 0]}
@@ -316,6 +318,13 @@
         def _(to=to):
             chunk_copy(to).start()
 
+    for special in (0, last):
+
+        @pl.when(z == special)
+        def _(special=special):
+            for w in sorted(far_side, key=lambda w: -min(abs(w - special), kv - abs(w - special))):
+                chunk_copy(w).start()
+
     for special, relay in relays.items():
 
         @pl.when((z > relay) & (z <= behind))
@@ -382,8 +391,13 @@
                     sq_copy(special).start()
                     chunk_copy(special).start()
 
-    middle_z = kv // 2
-    sides = {0: list(range(middle_z, 0, -1)), last: list(range(middle_z + 1, last))}
+    sides = {0: list(range(far_side[0] - 1, 0, -1)), last: list(range(far_side[-1] + 1, last))}
+    is_far = (z >= far_side[0]) & (z <= far_side[-1])
+
+    @pl.when(jnp.logical_not(is_far | is_special))
+    def _():
+        chunk_in[last] = jnp.zeros(chunk_in.shape[1:], BF16)
+
     for special, partner in ((last, 0), (0, last)):
 
         @pl.when(z == special)
@@ -399,12 +413,11 @@
                 chunk_out[w] = (chunk_out[w].astype(F32) + joint_in[w].astype(F32)).astype(BF16)
                 remote(chunk_out.at[w], chunk_in.at[0], rs_send.at[0], rs_recv.at[0], w, c).start()
 
-    def add_up(slots, joint):
+    def add_up(slots):
         sums = chunk_in[slots[0]].astype(F32)
         squares = sq_in[slots[0]]
         for w in slots[1:]:
-            if not (joint and w == last):
-                sums = sums + chunk_in[w].astype(F32)
+            sums = sums + chunk_in[w].astype(F32)
             squares = squares + sq_in[w]
         return sums, squares
 
@@ -413,8 +426,15 @@
     @pl.when(jnp.logical_not(is_special))
     def _():
         wait_all(sq_in, kv - 1, sq_recv.at[0])
-        wait_all(chunk_in, kv - 2, rs_recv.at[0])
-        sums, squares = add_up(order, True)
+        @pl.when(is_far)
+        def _():
+            wait_all(chunk_in, kv - 1, rs_recv.at[0])
+
+        @pl.when(jnp.logical_not(is_far))
+        def _():
+            wait_all(chunk_in, kv - 2, rs_recv.at[0])
+
+        sums, squares = add_up(order)
         total[pl.ds(0, 4 * group), :] = sums
         total[pl.ds(4 * group, seqs), :] = squares
 
@@ -422,7 +442,7 @@
     def _():
         wait_all(sq_in, len(near_last) + 1, sq_recv.at[0])
         wait_all(chunk_in, len(near_last) + 1, rs_recv.at[0])
-        sums, squares = add_up([*near_last, 0, last], False)
+        sums, squares = add_up([*near_last, 0, last])
         remote(relayed_out, relayed_in, relayed_send.at[0], relayed_recv.at[0], z, other).wait_recv()
         total[pl.ds(0, 4 * group), :] = sums + relayed_in[pl.ds(0, 4 * group), :]
         total[pl.ds(4 * group, seqs), :] = squares + relayed_in[pl.ds(4 * group, seqs), :]

time: 82.6 us -> 81.6 us (0.988)
  Pallas kernels: 81.8 us -> 80.8 us
    pallas_call x1, Pallas kernels: 80.8 us -> 79.9 us  [body(): pl.pallas_call(functools.partial(kernel, kv, tp), name='decode_step', out...]
where the time goes in v11:
time: 81.6 us; the launch traced here: 81.5 us
  Pallas kernels  80.8 us (99%)
    pallas_call x1, Pallas kernels, body(): pl.pallas_call(functools.partial(kernel, kv, tp), name='decode_step', out...  79.9 us

profile of v11, /device:TPU:65, one launch (start us, length us, event | category | flops | bytes accessed | tf_op | source)
XLA Modules:
  0.0 81.5 jit_solution(12973303885089037409)
XLA Ops:
  0.6 79.9 %decode_step.1 = (bf16[32,64]{1,0:T(8,128)(2,1)S(1)}, f32[2,8,128,128]{3,2,1,0:T(8,128)S(1)}) custom-call(bf16[32,64]{1,0:T(8,128)(2,1)} %tokens_hbm.1, f32[2,8,128,128]{3,2,1,0:T(8,128)} %past_state.1, f32[1,128]{1,0:T(1,128)} %bitcast.12, bf16[128,1024]{1,0:T(8,128)(2,1)} %w_query.1, bf16[128,1024]{1,0:T(8,128)(2,1)} %w_forget.1, ...), custom_call_target="tpu_custom_call" | custom-call | tf_op jit(solution)/shard_map/decode_step/pallas_call | solution.py:643
  80.5 1.0 %write_out.1 = (bf16[32,64]{1,0:T(8,128)(2,1)}, f32[2,8,128,128]{3,2,1,0:T(8,128)}) custom-call(bf16[32,64]{1,0:T(8,128)(2,1)S(1)} %get-tuple-element.4.result, f32[2,8,128,128]{3,2,1,0:T(8,128)S(1)} %get-tuple-element.5.new_state), custom_call_target="tpu_custom_call" | custom-call | tf_op jit(solution)/shard_map/write_out/pallas_call | solution.py:715

commit v12 on v11

--- a/solution.py
+++ b/solution.py
@@ -146,7 +146,7 @@
     last = kv - 1
     near_last = [w for w in range(kv - tp - 2, kv - 1)]
     middle_z = kv // 2
-    far_side = list(range(middle_z - 2, middle_z + 2))
+    far_side = list(range(middle_z - 3, middle_z + 3))
     relays = {0: kv // 4, last: near_last[0] - 1}
     behind = near_last[0] - 1
     listeners = {0: [relays[0], *near_last], last: [relays[last], *near_last, 0]}

time: 81.6 us -> 81 us (level)
  no operation moved by 1% of the time
where the time goes in v12:
time: 81 us; the launch traced here: 80.9 us
  Pallas kernels  80.2 us (99%)
    pallas_call x1, Pallas kernels, body(): pl.pallas_call(functools.partial(kernel, kv, tp), name='decode_step', out...  79.3 us

profile of v12, /device:TPU:65, one launch (start us, length us, event | category | flops | bytes accessed | tf_op | source)
XLA Modules:
  0.0 80.9 jit_solution(11128624973598451135)
XLA Ops:
  0.6 79.3 %decode_step.1 = (bf16[32,64]{1,0:T(8,128)(2,1)S(1)}, f32[2,8,128,128]{3,2,1,0:T(8,128)S(1)}) custom-call(bf16[32,64]{1,0:T(8,128)(2,1)} %tokens_hbm.1, f32[2,8,128,128]{3,2,1,0:T(8,128)} %past_state.1, f32[1,128]{1,0:T(1,128)} %bitcast.12, bf16[128,1024]{1,0:T(8,128)(2,1)} %w_query.1, bf16[128,1024]{1,0:T(8,128)(2,1)} %w_forget.1, ...), custom_call_target="tpu_custom_call" | custom-call | tf_op jit(solution)/shard_map/decode_step/pallas_call | solution.py:643
  79.9 1.0 %write_out.1 = (bf16[32,64]{1,0:T(8,128)(2,1)}, f32[2,8,128,128]{3,2,1,0:T(8,128)}) custom-call(bf16[32,64]{1,0:T(8,128)(2,1)S(1)} %get-tuple-element.4.result, f32[2,8,128,128]{3,2,1,0:T(8,128)S(1)} %get-tuple-element.5.new_state), custom_call_target="tpu_custom_call" | custom-call | tf_op jit(solution)/shard_map/write_out/pallas_call | solution.py:715

commit v13 on v12

--- a/solution.py
+++ b/solution.py
@@ -574,23 +574,28 @@
     for i in range(half_kv):
         at = slice(i * tp * feats, (i + 1) * tp * feats)
         top, bottom = terms[:half_rows, at], terms[half_rows:, at]
-        to = c * half_kv + i
         for to_c, message in (
             (0, jnp.where(low, top, halves_swapped(bottom))),
             (1, jnp.where(low, halves_swapped(top), bottom)),
         ):
-            n = 2 * i + to_c
-            terms_out[n] = message.astype(BF16)
-            copy = remote(terms_out.at[n], terms_in.at[z], term_send.at[0], term_recv.at[0], to, to_c)
-            to_self = jnp.logical_and(to == z, to_c == c)
-
-            @pl.when(jnp.logical_not(to_self))
-            def _(copy=copy):
-                copy.start()
-
-            @pl.when(to_self)
-            def _(n=n):
-                terms_in[z] = terms_out[n]
+            terms_out[tp * i + to_c] = message.astype(BF16)
+
+    def term_copy(to, to_c):
+        n = tp * (to - c * half_kv) + to_c
+        return remote(terms_out.at[n], terms_in.at[z], term_send.at[0], term_recv.at[0], to, to_c)
+
+    for d in far_first:
+        to = peer(d)
+
+        @pl.when(to // half_kv == c)
+        def _(to=to):
+            for to_c in range(tp):
+                term_copy(to, to_c).start()
+
+    @pl.when(kept_here)
+    def _():
+        term_copy(z, other).start()
+        terms_in[z] = terms_out[tp * (z - c * half_kv) + c]
 
     remote(wide_out, wide_in, pair_send.at[6], pair_recv.at[6], z, other).wait_send()
     wait_others(mid, mid_send.at[0], False)

time: 81 us -> 81.1 us (level)
  no operation moved by 1% of the time
where the time goes in v13:
time: 81.1 us; the launch traced here: 80.9 us
  Pallas kernels  80.3 us (99%)
    pallas_call x1, Pallas kernels, body(): pl.pallas_call(functools.partial(kernel, kv, tp), name='decode_step', out...  79.3 us

profile of v13, /device:TPU:65, one launch (start us, length us, event | category | flops | bytes accessed | tf_op | source)
XLA Modules:
  0.0 80.9 jit_solution(10638395559788170966)
XLA Ops:
  0.6 79.3 %decode_step.1 = (bf16[32,64]{1,0:T(8,128)(2,1)S(1)}, f32[2,8,128,128]{3,2,1,0:T(8,128)S(1)}) custom-call(bf16[32,64]{1,0:T(8,128)(2,1)} %tokens_hbm.1, f32[2,8,128,128]{3,2,1,0:T(8,128)} %past_state.1, f32[1,128]{1,0:T(1,128)} %bitcast.12, bf16[128,1024]{1,0:T(8,128)(2,1)} %w_query.1, bf16[128,1024]{1,0:T(8,128)(2,1)} %w_forget.1, ...), custom_call_target="tpu_custom_call" | custom-call | tf_op jit(solution)/shard_map/decode_step/pallas_call | solution.py:648
  80.0 1.0 %write_out.1 = (bf16[32,64]{1,0:T(8,128)(2,1)}, f32[2,8,128,128]{3,2,1,0:T(8,128)}) custom-call(bf16[32,64]{1,0:T(8,128)(2,1)S(1)} %get-tuple-element.4.result, f32[2,8,128,128]{3,2,1,0:T(8,128)S(1)} %get-tuple-element.5.new_state), custom_call_target="tpu_custom_call" | custom-call | tf_op jit(solution)/shard_map/write_out/pallas_call | solution.py:720

commit v14 on v12

--- a/solution.py
+++ b/solution.py
@@ -147,7 +147,7 @@
     near_last = [w for w in range(kv - tp - 2, kv - 1)]
     middle_z = kv // 2
     far_side = list(range(middle_z - 3, middle_z + 3))
-    relays = {0: kv // 4, last: near_last[0] - 1}
+    relays = {0: kv // 4 - 1, last: near_last[0] - 1}
     behind = near_last[0] - 1
     listeners = {0: [relays[0], *near_last], last: [relays[last], *near_last, 0]}
     far_first = sorted(range(1, kv), key=lambda d: -min(d, kv - d))

time: 81 us -> 81.1 us (level)
  no operation moved by 1% of the time
where the time goes in v14:
time: 81.1 us; the launch traced here: 80.9 us
  Pallas kernels  80.3 us (99%)
    pallas_call x1, Pallas kernels, body(): pl.pallas_call(functools.partial(kernel, kv, tp), name='decode_step', out...  79.3 us

profile of v14, /device:TPU:65, one launch (start us, length us, event | category | flops | bytes accessed | tf_op | source)
XLA Modules:
  0.0 80.9 jit_solution(17523022190384611590)
XLA Ops:
  0.6 79.3 %decode_step.1 = (bf16[32,64]{1,0:T(8,128)(2,1)S(1)}, f32[2,8,128,128]{3,2,1,0:T(8,128)S(1)}) custom-call(bf16[32,64]{1,0:T(8,128)(2,1)} %tokens_hbm.1, f32[2,8,128,128]{3,2,1,0:T(8,128)} %past_state.1, f32[1,128]{1,0:T(1,128)} %bitcast.12, bf16[128,1024]{1,0:T(8,128)(2,1)} %w_query.1, bf16[128,1024]{1,0:T(8,128)(2,1)} %w_forget.1, ...), custom_call_target="tpu_custom_call" | custom-call | tf_op jit(solution)/shard_map/decode_step/pallas_call | solution.py:643
  79.9 1.0 %write_out.1 = (bf16[32,64]{1,0:T(8,128)(2,1)}, f32[2,8,128,128]{3,2,1,0:T(8,128)}) custom-call(bf16[32,64]{1,0:T(8,128)(2,1)S(1)} %get-tuple-element.4.result, f32[2,8,128,128]{3,2,1,0:T(8,128)S(1)} %get-tuple-element.5.new_state), custom_call_target="tpu_custom_call" | custom-call | tf_op jit(solution)/shard_map/write_out/pallas_call | solution.py:715
